TPU v7x, 32 devices: a whole 2x2x4 slice. The times are simulated.
32 devices in a mesh: tp: 32 (over z, y, x, core).
Axes of the slice: x: 2, y: 2, z: 4, core: 2. Of those that a mesh axis runs over, the one named last changes fastest.
Arguments:
- tokens: bfloat16 [32, 8, 4096], P('tp'), may hold values from -6 to 6
- block_norm_gain: float32 [2, 4096], replicated, may hold values from 0.1 to 1.9
- receptance_weight: bfloat16 [2, 32, 4096, 64], P(None, 'tp'), may hold values from -0.09375 to 0.09375
- key_weight: bfloat16 [2, 32, 4096, 64], P(None, 'tp'), may hold values from -0.09375 to 0.09375
- value_weight: bfloat16 [2, 32, 4096, 64], P(None, 'tp'), may hold values from -0.09375 to 0.09375
- decay_weight: bfloat16 [2, 32, 4096, 64], P(None, 'tp'), may hold values from -0.09375 to 0.09375
- learning_rate_weight: bfloat16 [2, 32, 4096, 64], P(None, 'tp'), may hold values from -0.09375 to 0.09375
- gate_weight: bfloat16 [2, 32, 4096, 64], P(None, 'tp'), may hold values from -0.09375 to 0.09375
- decay_bias_fixed: float32 [2, 2048], replicated, may hold values from -5 to 2
- self_token_weight: float32 [2, 2048], replicated, may hold values from -1.5 to 1.5
- readout_norm_gain: float32 [2, 2048], replicated, may hold values from 0.1 to 1.9
- output_weight: bfloat16 [2, 32, 64, 4096], P(None, 'tp'), may hold values from -0.125 to 0.125
- state: float32 [2, 32, 256, 4096], P(None, 'tp'), may hold values from -3 to 3
Outputs:
- mixed: bfloat16 [32, 8, 4096], P('tp')
- new_state: float32 [2, 32, 256, 4096], P(None, 'tp')
All inputs are finite; a program needn't handle non-finite values.
Results may differ from a plain program's by a relative error of at most 0.018.
Values may be sent and summed in bfloat16 or wider, within the bound.
No kernel may reach another device: no remote copies, remote signals or barrier semaphores. Data moves between devices by JAX's collectives and lax.ppermute only.
A program may use at most 128 MiB of HBM per device.

v0:
```python
from functools import partial

import jax
import jax.numpy as jnp
from jax import lax
from jax.experimental import pallas as pl
from jax.experimental.pallas import tpu as pltpu
from jax.sharding import PartitionSpec as P


D = 4096


RMS_EPS = 1e-06
GROUP_EPS = 0.00064


def swapped(shard, axis, stride):
    return lax.ppermute(shard, axis, [(i, i ^ 1 << stride) for i in range(lax.axis_size(axis))])


def for_sending(shard):

    def short(part):
        return part.astype(jnp.bfloat16) if part.dtype == jnp.float32 else part

    return jax.tree.map(short, shard)


def recurrent_update(
    layer_state,
    receptance_vector,
    key_vector,
    value_vector,
    decay_logits,
    learning_rate_logits,
    gate_logits,
    decay_constant,
    self_term_scale,
    head_gain_slice,
):
    highest = lax.Precision.HIGHEST
    shrink = jnp.exp(-jnp.exp(-jax.nn.softplus(-(decay_constant + decay_logits)) - 0.5))
    rate = jax.nn.sigmoid(learning_rate_logits)
    normed = key_vector * lax.rsqrt(jnp.sum(key_vector * key_vector, -1, keepdims=True) + 1.0)
    removed = jnp.einsum("...ij,...j->...i", layer_state, normed, precision=highest)
    layer_state = (
        layer_state * shrink[..., None, :]
        - removed[..., :, None] * (normed * rate)[..., None, :]
        + value_vector[..., :, None] * (key_vector * rate)[..., None, :]
    )
    readout = jnp.einsum("...ij,...j->...i", layer_state, receptance_vector, precision=highest)
    center = jnp.mean(readout, -1, keepdims=True)
    spread = jnp.mean(jnp.square(readout - center), -1, keepdims=True)
    normed_output = (readout - center) * lax.rsqrt(spread + GROUP_EPS) * head_gain_slice
    self_term = (
        jnp.sum(receptance_vector * key_vector * self_term_scale, -1, keepdims=True) * value_vector
    )
    return (
        ((normed_output + self_term) * jax.nn.sigmoid(gate_logits)).astype(jnp.bfloat16),
        layer_state,
    )


def double_gather(piece, position, first_bit, count, mover):
    for offset in range(count):
        which_bit = first_bit + offset
        partner = mover(piece, which_bit)
        lower_self = position >> which_bit & 1 == 0
        piece = jnp.where(
            lower_self, jnp.concatenate([piece, partner], 0), jnp.concatenate([partner, piece], 0)
        )
    return piece


def halve_sum(members, position, first_bit, count, mover):
    for offset in reversed(range(count)):
        which_bit = first_bit + offset
        upper_self = position >> which_bit & 1 == 1
        sends = tuple(
            (
                jnp.where(
                    upper_self, member[: member.shape[0] // 2], member[member.shape[0] // 2 :]
                )
                for member in members
            )
        )
        keeps = tuple(
            (
                jnp.where(
                    upper_self, member[member.shape[0] // 2 :], member[: member.shape[0] // 2]
                )
                for member in members
            )
        )
        arrived = mover(sends, which_bit)
        members = tuple((kept + got for kept, got in zip(keeps, arrived)))
    return members


def on_device_blocked(
    tokens,
    block_norm_gain,
    receptance_weight,
    key_weight,
    value_weight,
    decay_weight,
    learning_rate_weight,
    gate_weight,
    decay_bias_fixed,
    self_token_weight,
    readout_norm_gain,
    output_weight,
    state,
):
    columns_dev = tokens.shape[2]
    row_blocks = D // columns_dev
    low_bits = row_blocks.bit_length() - 1
    head_count = lax.axis_size("tp") // row_blocks
    high_bits = head_count.bit_length() - 1
    position = lax.axis_index("tp")
    head_index = position // row_blocks
    row_block = position % row_blocks
    head_size = receptance_weight.shape[3]
    seq_tile = tokens.shape[1]
    move_rows = lambda payload, which_bit: swapped(payload, "tp", which_bit)
    move_proj = lambda payload, which_bit: swapped(payload, "tp", which_bit)
    move_outs = lambda payload, which_bit: jax.tree.map(
        lambda part, own: part.astype(own.dtype),
        swapped(for_sending(payload), "tp", which_bit),
        payload,
    )
    move_split = lambda payload, which_bit: jax.tree.map(
        lambda part, own: part.astype(own.dtype),
        swapped(for_sending(payload), "tp", which_bit),
        payload,
    )

    def mixer(columns, layer_index):
        gain_cols = lax.dynamic_slice_in_dim(
            block_norm_gain[layer_index], row_block * columns_dev, columns_dev
        )
        wide = columns.astype(jnp.float32)
        scaled = (wide * gain_cols).astype(jnp.bfloat16)
        squares = jnp.sum(wide * wide, axis=1)
        weights = jnp.concatenate(
            [
                receptance_weight[layer_index, 0],
                key_weight[layer_index, 0],
                value_weight[layer_index, 0],
                decay_weight[layer_index, 0],
                learning_rate_weight[layer_index, 0],
                gate_weight[layer_index, 0],
            ],
            axis=1,
        )
        partial_value = jnp.dot(scaled, weights, preferred_element_type=jnp.float32)
        summed, total_sq = halve_sum((partial_value, squares), position, 0, low_bits, move_proj)
        projected = summed * lax.rsqrt(total_sq / D + RMS_EPS)[:, None]
        output_pieces = jnp.split(projected, 6, axis=1)

        def head_columns(table):
            return lax.dynamic_slice_in_dim(table[layer_index], head_index * head_size, head_size)

        layer_state = state[layer_index, 0].reshape(-1, head_size, head_size)
        out_tile, layer_state = recurrent_update(
            layer_state,
            *output_pieces,
            head_columns(decay_bias_fixed),
            head_columns(self_token_weight),
            head_columns(readout_norm_gain)
        )
        out_all = double_gather(out_tile, position, 0, low_bits, move_outs)
        branch = jnp.dot(out_all, output_weight[layer_index, 0], preferred_element_type=jnp.float32)
        return (branch, layer_state.reshape(layer_state.shape[0], head_size * head_size))

    columns = double_gather(tokens[0], position, low_bits, high_bits, move_rows)
    first_branch, first_memory = mixer(columns, 0)
    (tile_sum,) = halve_sum((first_branch,), position, low_bits, high_bits, move_split)
    tile_one = (tokens[0].astype(jnp.float32) + tile_sum).astype(jnp.bfloat16)
    columns = double_gather(tile_one, position, low_bits, high_bits, move_rows)
    second_branch, second_memory = mixer(columns, 1)
    (tile_sum,) = halve_sum((second_branch,), position, low_bits, high_bits, move_split)
    resid_rows = lax.dynamic_slice_in_dim(columns, head_index * seq_tile, seq_tile, 0)
    mixed = (resid_rows.astype(jnp.float32) + tile_sum).astype(jnp.bfloat16)
    new_state = jnp.stack([first_memory, second_memory])[:, None]
    return (mixed[None], new_state)


CORES = 2
PLANE = 4
STATE_ROWS = 64


def moved(part, mask):
    return lax.ppermute(part, "tp", [(i, i ^ mask) for i in range(lax.axis_size("tp"))])


def near(part):
    return pltpu.with_memory_space_constraint(part, pltpu.VMEM)


def far(part):
    return pltpu.with_memory_space_constraint(part, pltpu.HBM)


def slots(place_ref, rows, seq_tile):
    chips = rows // seq_tile // CORES
    levels = chips // PLANE
    for off_core in range(CORES):
        for apart in range(PLANE):
            for level in range(levels):
                chip = place_ref[0] ^ (apart + PLANE * level)
                tile = chip * CORES + (place_ref[1] ^ off_core)
                yield pl.multiple_of(tile * seq_tile, seq_tile)


def load_kernel(place_ref, *refs, layer, layers, count, head_size, seq_tile):
    arrived, loaded = refs[-2:]
    refs = refs[:-2]
    split = (len(refs) + count - (layers if count else 0)) // 2
    (state_ref, *sources), (rows_ref, *targets) = refs[:split], refs[split:]
    pairs = [
        (ref.at[at_layer, 0], targets[at_layer].at[at * head_size : (at + 1) * head_size, :])
        for at_layer in range(layers if count else 0)
        for at, ref in enumerate(sources[:count])
    ] + list(zip(sources[count:], targets[layers:]))
    copies = [
        pltpu.make_async_copy(source, target, arrived.at[at])
        for at, (source, target) in enumerate(pairs)
    ]
    for copy in copies:
        copy.start()
    for slot, at in enumerate(slots(place_ref, rows_ref.shape[0], seq_tile)):
        pltpu.make_async_copy(
            state_ref.at[layer, 0, pl.ds(at, seq_tile)],
            rows_ref.at[slot * seq_tile : (slot + 1) * seq_tile],
            loaded,
        ).start()
    for copy in copies:
        copy.wait()
    pltpu.make_async_copy(state_ref.at[layer, 0], rows_ref, loaded).wait()


def load(place, state, layer, weights=(), tables=()):
    layers = state.shape[0]
    seqs = state.shape[2]
    outs = [pltpu.VMEM(state.shape[2:], state.dtype)]
    head_size = 0
    if weights:
        _, _, head_size, columns = weights[0].shape
        outs += [pltpu.VMEM((len(weights) * head_size, columns), jnp.bfloat16)] * layers
    outs += [pltpu.VMEM(table.shape, table.dtype) for table in tables]
    sources = [state, *weights, *tables]
    loaded = pl.pallas_call(
        partial(
            load_kernel,
            layer=layer,
            layers=layers,
            count=len(weights),
            head_size=head_size,
            seq_tile=seqs // lax.axis_size("tp"),
        ),
        in_specs=[pl.BlockSpec(memory_space=pltpu.SMEM)]
        + [pl.BlockSpec(memory_space=pltpu.HBM)] * len(sources),
        out_specs=[pl.BlockSpec(memory_space=pltpu.VMEM)] * len(outs),
        out_shape=outs,
        scratch_shapes=[
            pltpu.SemaphoreType.DMA((layers * len(weights) + len(tables) + 1,)),
            pltpu.SemaphoreType.DMA,
        ],
        compiler_params=pltpu.CompilerParams(vmem_limit_bytes=1 << 20),
    )(place, *[far(source) for source in sources])
    return tuple(loaded)


def front_kernel(place_ref, *refs, piece_rows, head_size, layer):
    pieces = refs[: len(piece_rows)]
    (
        gain_ref,
        bias_ref,
        self_ref,
        readout_ref,
        weights_ref,
        rows_ref,
        out_ref,
        vec_ref,
        scaled_ref,
        fold_ref,
    ) = refs[len(piece_rows) :]
    wide = 2 * head_size
    seqs, columns = rows_ref.shape
    core = place_ref[1]

    def own(ref):
        row = ref[layer : layer + 1, pl.ds(pl.multiple_of(place_ref[0] * wide, wide), wide)]
        return jnp.where(core == 0, row[:, :head_size], row[:, head_size:])

    gain = gain_ref[layer : layer + 1, :]
    sums = [None] * (seqs // 16)
    for ref, rows in zip(pieces, piece_rows):
        for at, row in enumerate(rows):
            part = ref[at * 16 : at * 16 + 16, :].astype(jnp.float32)
            scaled_ref[row : row + 16, :] = (part * gain).astype(jnp.bfloat16)
            sums[row // 16] = jnp.sum(part * part, axis=1, keepdims=True)
    projected = lax.dot_general(
        scaled_ref[...],
        weights_ref[...],
        (((1,), (1,)), ((), ())),
        preferred_element_type=jnp.float32,
    )
    at_row = lax.broadcasted_iota(jnp.int32, fold_ref.shape, 0) >> (head_size.bit_length() - 1)
    at_lane = lax.broadcasted_iota(jnp.int32, fold_ref.shape, 1)
    fold_ref[...] = jnp.where(at_row == at_lane, 1.0, 0.0).astype(jnp.bfloat16)
    total = jnp.concatenate(sums, 0)
    projected = projected * lax.rsqrt(total / scaled_ref.shape[1] + RMS_EPS)
    r, k, v, p, q, g = [projected[:, at * head_size : (at + 1) * head_size] for at in range(6)]
    decay = jnp.exp(jax.nn.sigmoid(own(bias_ref) + p) * (-(2.718281828459045**-0.5)))
    rate = jax.nn.sigmoid(q)
    kn = k * lax.rsqrt(jnp.sum(k * k, -1, keepdims=True) + 1.0)
    decay_r = decay * r
    twice = lambda part: jnp.concatenate([part, part], 1)
    kn_wide, decay_r_wide = twice(kn), twice(decay_r)
    repeats = columns // wide
    removed, kept = [], []
    for block in range(seqs // STATE_ROWS):
        span = slice(block * STATE_ROWS, (block + 1) * STATE_ROWS)
        rows = rows_ref[span, :]
        by_kn = (rows * jnp.tile(kn_wide[span], (1, repeats))).astype(jnp.bfloat16)
        by_r = (rows * jnp.tile(decay_r_wide[span], (1, repeats))).astype(jnp.bfloat16)
        both = jnp.dot(
            jnp.concatenate([by_kn, by_r], 0), fold_ref[...], preferred_element_type=jnp.float32
        )
        removed.append(both[:STATE_ROWS, :head_size])
        kept.append(both[STATE_ROWS:, :head_size])
    removed, kept = jnp.concatenate(removed, 0), jnp.concatenate(kept, 0)
    kn_rate = kn * rate
    k_rate = k * rate
    row_sum = lambda part: jnp.sum(part, -1, keepdims=True)
    readout = kept - removed * row_sum(kn_rate * r) + v * row_sum(k_rate * r)
    center = jnp.mean(readout, -1, keepdims=True)
    spread = jnp.mean(jnp.square(readout - center), -1, keepdims=True)
    normed = (readout - center) * lax.rsqrt(spread + GROUP_EPS) * own(readout_ref)
    out = (normed + row_sum(r * k * own(self_ref)) * v) * jax.nn.sigmoid(g)
    out_ref[...] = out.astype(jnp.bfloat16)
    for at, pair in enumerate(
        (twice(decay), twice(kn_rate), twice(k_rate), jnp.concatenate([v, removed], 1))
    ):
        vec_ref[:, at * wide : (at + 1) * wide] = pair


def front(place, pieces, piece_rows, gain, tables, packed, rows, layer):
    seqs, columns = rows.shape
    head_size = packed.shape[0] // 6
    wide = 2 * head_size
    vmem = pl.BlockSpec(memory_space=pltpu.VMEM)
    return pl.pallas_call(
        partial(front_kernel, piece_rows=piece_rows, head_size=head_size, layer=layer),
        in_specs=[pl.BlockSpec(memory_space=pltpu.SMEM)]
        + [vmem] * (len(pieces) + 3 + len(tables)),
        out_specs=[vmem, vmem],
        scratch_shapes=[
            pltpu.VMEM((seqs, D), jnp.bfloat16),
            pltpu.VMEM((columns, wide), jnp.bfloat16),
        ],
        out_shape=[
            jax.ShapeDtypeStruct((seqs, head_size), jnp.bfloat16),
            jax.ShapeDtypeStruct((seqs, 4 * wide), jnp.float32),
        ],
        compiler_params=pltpu.CompilerParams(vmem_limit_bytes=36 << 20),
    )(place, *[near(piece) for piece in pieces], near(gain), *[near(t) for t in tables], near(packed), near(rows))


def update_kernel(place_ref, vec_ref, rows_ref, *refs, seq_tile, head_size, layer):
    out_ref, spread_ref, results_ref, written = refs[-4:]
    wide = 2 * head_size
    seqs, columns = rows_ref.shape
    repeats = columns // wide
    at_row = lax.broadcasted_iota(jnp.int32, spread_ref.shape, 0) & (head_size - 1)
    at_lane = lax.broadcasted_iota(jnp.int32, spread_ref.shape, 1) >> (head_size.bit_length() - 1)
    spread_ref[...] = jnp.where(at_row == at_lane, 1.0, 0.0).astype(jnp.bfloat16)
    tiles = list(slots(place_ref, seqs, seq_tile))
    per_block = STATE_ROWS // seq_tile
    for block in range(seqs // STATE_ROWS):
        span = slice(block * STATE_ROWS, (block + 1) * STATE_ROWS)
        pair = vec_ref[span, 3 * wide :]
        high = pair.astype(jnp.bfloat16)
        low = (pair - high.astype(jnp.float32)).astype(jnp.bfloat16)

        def spread(at):
            lanes = slice(at * head_size, (at + 1) * head_size)
            both = jnp.concatenate([high[:, lanes], low[:, lanes]], 1)
            return jnp.dot(both, spread_ref[...], preferred_element_type=jnp.float32)

        row = lambda at: jnp.tile(vec_ref[span, at * wide : (at + 1) * wide], (1, repeats))
        results_ref[span, :] = rows_ref[span, :] * row(0) - spread(1) * row(1) + spread(0) * row(2)
        for slot in range(block * per_block, (block + 1) * per_block):
            pltpu.make_async_copy(
                results_ref.at[slot * seq_tile : (slot + 1) * seq_tile],
                out_ref.at[layer, 0, pl.ds(tiles[slot], seq_tile)],
                written.at[block],
            ).start()
    for block in range(seqs // STATE_ROWS):
        span = slice(block * STATE_ROWS, (block + 1) * STATE_ROWS)
        pltpu.make_async_copy(
            results_ref.at[span], out_ref.at[layer, 0, :STATE_ROWS], written.at[block]
        ).wait()


def update(place, vec, rows, previous, shape, layer):
    seqs, columns = rows.shape
    head_size = vec.shape[1] // 8
    vmem = pl.BlockSpec(memory_space=pltpu.VMEM)
    hbm = pl.BlockSpec(memory_space=pltpu.HBM)
    more = [previous] if previous is not None else []
    return pl.pallas_call(
        partial(
            update_kernel,
            seq_tile=seqs // lax.axis_size("tp"),
            head_size=head_size,
            layer=layer,
        ),
        in_specs=[pl.BlockSpec(memory_space=pltpu.SMEM), vmem, vmem] + [hbm] * len(more),
        out_specs=hbm,
        scratch_shapes=[
            pltpu.VMEM((2 * head_size, columns), jnp.bfloat16),
            pltpu.VMEM((seqs, columns), jnp.float32),
            pltpu.SemaphoreType.DMA((seqs // STATE_ROWS,)),
        ],
        out_shape=jax.ShapeDtypeStruct(shape, rows.dtype),
        input_output_aliases={3: 0} if more else {},
        compiler_params=pltpu.CompilerParams(vmem_limit_bytes=24 << 20),
    )(place, near(vec), near(rows), *more)


def gather_tiles(tile, levels):
    step = CORES * PLANE
    groups = [jnp.concatenate([tile, moved(tile, step)], 0)]
    if levels > 2:
        distant = [moved(tile, step * apart) for apart in range(2, levels)]
        groups.append(jnp.concatenate(distant, 0))
    rows = tile.shape[0]
    half = PLANE * levels * rows
    part = lambda q, at, size: [q * levels * rows + at + r for r in range(0, size, 16)]
    pieces, places, swaps = [], [], []
    start = 0
    for group in groups:
        order = (3, 1, 2)
        got = [moved(group, CORES * q) for q in order]
        pieces += [group] + got
        places += [part(q, start, group.shape[0]) for q in (0, *order)]
        swaps.append((got, [r for q in order for r in part(q, start, group.shape[0])]))
        start += group.shape[0]
    swaps.insert(0, (groups, part(0, 0, start)))
    for parts, spots in swaps:
        pieces.append(moved(jnp.concatenate(parts, 0), 1))
        places.append([half + r for r in spots])
    return pieces, places


def sum_tiles(parts, levels, during):
    rows = parts.shape[0] // (PLANE * levels)
    block = levels * rows
    sends = parts.astype(jnp.bfloat16)
    got = [moved(sends[q * block : (q + 1) * block], CORES * q) for q in (3, 1, 2)]
    *got, during = lax.optimization_barrier((*got, during))
    summed = parts[:block] + sum(part.astype(jnp.float32) for part in got)
    sends = summed.astype(jnp.bfloat16)
    got = [
        moved(sends[at * rows : (at + 1) * rows], CORES * PLANE * at) for at in range(1, levels)
    ]
    return summed[:rows] + sum(part.astype(jnp.float32) for part in got), during


def on_device_whole(
    tokens,
    block_norm_gain,
    receptance_weight,
    key_weight,
    value_weight,
    decay_weight,
    learning_rate_weight,
    gate_weight,
    decay_bias_fixed,
    self_token_weight,
    readout_norm_gain,
    output_weight,
    state,
):
    devices = lax.axis_size("tp")
    levels = devices // (CORES * PLANE)
    position = lax.axis_index("tp")
    place = jnp.stack([position // CORES, position % CORES]).astype(jnp.int32)
    weights = [
        jnp.swapaxes(w, 2, 3)
        for w in (
            receptance_weight,
            key_weight,
            value_weight,
            decay_weight,
            learning_rate_weight,
            gate_weight,
        )
    ]
    tables = (decay_bias_fixed, self_token_weight, readout_norm_gain)
    own_out = output_weight[:, 0]
    other_out = moved(own_out, 1)

    tile, place = lax.optimization_barrier((tokens[0], place))
    new_state = None
    layers = state.shape[0]
    for layer in range(layers):
        pieces, places = gather_tiles(tile, levels)
        if layer == 0:
            loaded = load(place, state, layer, weights, (block_norm_gain, *tables))
            packed, (gain, *tables) = loaded[1 : 1 + layers], loaded[1 + layers :]
        else:
            loaded = load(place, state, layer)
        rows = loaded[0]
        out, vec = front(place, pieces, places, gain, tables, packed[layer], rows, layer)
        half = out.shape[0] // CORES
        parts = jnp.dot(out[:half], own_out[layer], preferred_element_type=jnp.float32)
        parts += jnp.dot(moved(out[half:], 1), other_out[layer], preferred_element_type=jnp.float32)
        parts, vec = lax.optimization_barrier((parts, vec))
        new_state = update(place, vec, rows, new_state, state.shape, layer)
        total, new_state = sum_tiles(parts, levels, new_state)
        tile = (tile.astype(jnp.float32) + total).astype(jnp.bfloat16)
    return (tile[None], new_state)


def on_device(tokens, *rest):
    if tokens.shape[2] == D and lax.axis_size("tp") >= 16:
        return on_device_whole(tokens, *rest)
    return on_device_blocked(tokens, *rest)


def solution(mesh):
    return jax.shard_map(
        on_device,
        mesh=mesh,
        in_specs=(
            P("tp", None, None),
            P(),
            P(None, "tp", None, None),
            P(None, "tp", None, None),
            P(None, "tp", None, None),
            P(None, "tp", None, None),
            P(None, "tp", None, None),
            P(None, "tp", None, None),
            P(),
            P(),
            P(),
            P(None, "tp", None, None),
            P(None, "tp", None, None),
        ),
        out_specs=(P("tp", None, None), P(None, "tp", None, None)),
        check_vma=False,
    )
```

profile of v0, /device:TPU:0, one launch (start us, length us, event | category | flops | bytes accessed | tf_op | source)
XLA Modules:
  0.0 121.2 jit_solution(18382888575886503124)
XLA Ops:
  0.7 4.1 %collective-permute-start.4 = (bf16[8,4096]{1,0:T(8,128)(2,1)}, bf16[8,4096]{1,0:T(8,128)(2,1)S(1)}, u32[]{:S(2)}, u32[]{:S(2)}) collective-permute-start(bf16[8,4096]{1,0:T(8,128)(2,1)} %bitcast.33), channel_id=1, source_target_pairs={{0,16},{1,17},{2,18},{3,19},{4,20},{5,21},{6,22},{7,23},{8,24},{9,... | collective-permute-start | bytes 196616 | tf_op jit(solution)/shard_map/ppermute | solution.py:196
  7.3 1.5 %collective-permute-done.4 = bf16[8,4096]{1,0:T(8,128)(2,1)S(1)} collective-permute-done((bf16[8,4096]{1,0:T(8,128)(2,1)}, bf16[8,4096]{1,0:T(8,128)(2,1)S(1)}, u32[]{:S(2)}, u32[]{:S(2)}) %collective-permute-start.4) | collective-permute-done | bytes 65568 | tf_op jit(solution)/shard_map/ppermute | solution.py:196
  8.7 2.4 %collective-permute-done.5 = bf16[8,4096]{1,0:T(8,128)(2,1)S(1)} collective-permute-done((bf16[8,4096]{1,0:T(8,128)(2,1)}, bf16[8,4096]{1,0:T(8,128)(2,1)S(1)}, u32[]{:S(2)}, u32[]{:S(2)}) %collective-permute-start.5) | collective-permute-done | bytes 65568 | tf_op jit(solution)/shard_map/ppermute | solution.py:196
  11.2 2.5 %collective-permute-start.6 = (bf16[16,4096]{1,0:T(8,128)(2,1)S(1)}, bf16[16,4096]{1,0:T(8,128)(2,1)S(1)}, u32[]{:S(2)}, u32[]{:S(2)}) collective-permute-start(bf16[16,4096]{1,0:T(8,128)(2,1)S(1)} %constant_dynamic-update-slice_fusion.2.refs_4_), channel_id=1, source_target_pairs={{0,6},{1,7},{2,4},{3,5},{4,2},{5,3},{6,0},{7,1},{8,14},{9,15},{10,... | collective-permute-start | bytes 393224 | tf_op jit(solution)/shard_map/ppermute | solution.py:196
  14.7 2.5 %collective-permute-start.1 = (bf16[16,4096]{1,0:T(8,128)(2,1)S(1)}, bf16[16,4096]{1,0:T(8,128)(2,1)S(1)}, u32[]{:S(2)}, u32[]{:S(2)}) collective-permute-start(bf16[16,4096]{1,0:T(8,128)(2,1)S(1)} %constant_dynamic-update-slice_fusion.refs_0_), channel_id=1, source_target_pairs={{0,6},{1,7},{2,4},{3,5},{4,2},{5,3},{6,0},{7,1},{8,14},{9,15},{10,... | collective-permute-start | bytes 393224 | tf_op jit(solution)/shard_map/ppermute | solution.py:196
  18.6 1.5 %collective-permute-start.2 = (bf16[16,4096]{1,0:T(8,128)(2,1)S(1)}, bf16[16,4096]{1,0:T(8,128)(2,1)S(1)}, u32[]{:S(2)}, u32[]{:S(2)}) collective-permute-start(bf16[16,4096]{1,0:T(8,128)(2,1)S(1)} %constant_dynamic-update-slice_fusion.refs_0_), channel_id=1, source_target_pairs={{0,2},{1,3},{2,0},{3,1},{4,6},{5,7},{6,4},{7,5},{8,10},{9,11},{10,... | collective-permute-start | bytes 393224 | tf_op jit(solution)/shard_map/ppermute | solution.py:196
  23.0 1.4 %collective-permute-done.2.refs_2_ = bf16[16,4096]{1,0:T(8,128)(2,1)S(1)} collective-permute-done((bf16[16,4096]{1,0:T(8,128)(2,1)S(1)}, bf16[16,4096]{1,0:T(8,128)(2,1)S(1)}, u32[]{:S(2)}, u32[]{:S(2)}) %collective-permute-start.2) | collective-permute-done | bytes 131104 | tf_op jit(solution)/shard_map/ppermute | solution.py:196
  24.4 1.9 %collective-permute-done.3.refs_3_ = bf16[16,4096]{1,0:T(8,128)(2,1)S(1)} collective-permute-done((bf16[16,4096]{1,0:T(8,128)(2,1)S(1)}, bf16[16,4096]{1,0:T(8,128)(2,1)S(1)}, u32[]{:S(2)}, u32[]{:S(2)}) %collective-permute-start.3) | collective-permute-done | bytes 131104 | tf_op jit(solution)/shard_map/ppermute | solution.py:196
  27.0 4.8 %shard_map.140 = (f32[256,4096]{1,0:T(8,128)S(1)}, bf16[384,4096]{1,0:T(8,128)(2,1)S(1)}, bf16[384,4096]{1,0:T(8,128)(2,1)S(1)}, f32[2,4096]{1,0:T(2,128)S(1)}, ...) custom-call(s32[2]{0:T(128)S(1)} %pad_add_fusion.place_ref, f32[2,1,256,4096]{3,2,1,0:T(8,128)} %refs_0_.3, ...), custom_call_target="tpu_custom_call" | custom-call | tf_op jit(solution)/shard_map/pallas_call | solution.py:255
  31.8 4.7 %shard_map.141 = (bf16[256,64]{1,0:T(8,128)(2,1)S(1)}, f32[256,512]{1,0:T(8,128)S(1)}) custom-call(s32[2]{0:T(128)S(1)} %pad_add_fusion.place_ref, bf16[16,4096]{1,0:T(8,128)(2,1)S(1)} %constant_dynamic-update-slice_fusion.refs_0_, bf16[16,4096]{1,0:T(8,128)(2,1)S(1)} %collective-permute-done.1.refs_1_, bf16[16,4096]{1,0:T(8,128)(2,1)S(1)} %collective-permute-done.2.refs_2_, ...), custom_call_target="tpu_custom_call" | custom-call | tf_op jit(solution)/shard_map/pallas_call | solution.py:357
  38.9 1.5 %collective-permute-start.14 = (bf16[32,4096]{1,0:T(8,128)(2,1)S(1)}, bf16[32,4096]{1,0:T(8,128)(2,1)S(1)}, u32[]{:S(2)}, u32[]{:S(2)}) collective-permute-start(bf16[32,4096]{1,0:T(8,128)(2,1)S(1)} %get-tuple-element.61), channel_id=1, source_target_pairs={{0,6},{1,7},{2,4},{3,5},{4,2},{5,3},{6,0},{7,1},{8,14},{9,15},{10,... | collective-permute-start | bytes 786440 | tf_op jit(solution)/shard_map/ppermute | solution.py:196
  41.0 1.5 %collective-permute-start.16 = (bf16[32,4096]{1,0:T(8,128)(2,1)S(1)}, bf16[32,4096]{1,0:T(8,128)(2,1)S(1)}, u32[]{:S(2)}, u32[]{:S(2)}) collective-permute-start(bf16[32,4096]{1,0:T(8,128)(2,1)S(1)} %get-tuple-element.59), channel_id=1, source_target_pairs={{0,4},{1,5},{2,6},{3,7},{4,0},{5,1},{6,2},{7,3},{8,12},{9,13},{10,... | collective-permute-start | bytes 786440 | tf_op jit(solution)/shard_map/ppermute | solution.py:196
  42.5 3.6 %shard_map.142.refs_0_ = f32[2,1,256,4096]{3,2,1,0:T(8,128)} custom-call(s32[2]{0:T(128)S(1)} %pad_add_fusion.place_ref, f32[256,512]{1,0:T(8,128)S(1)} %get-tuple-element.38.vec_ref, f32[256,4096]{1,0:T(8,128)S(1)} %get-tuple-element.34.refs_16_.rows_ref), custom_call_target="tpu_custom_call" | custom-call | tf_op jit(solution)/shard_map/pallas_call | solution.py:416
  46.1 3.0 %collective-permute-done.14 = bf16[32,4096]{1,0:T(8,128)(2,1)S(1)} collective-permute-done((bf16[32,4096]{1,0:T(8,128)(2,1)S(1)}, bf16[32,4096]{1,0:T(8,128)(2,1)S(1)}, u32[]{:S(2)}, u32[]{:S(2)}) %collective-permute-start.14) | collective-permute-done | bytes 262176 | tf_op jit(solution)/shard_map/ppermute | solution.py:196
  49.1 3.9 %collective-permute-done.15 = bf16[32,4096]{1,0:T(8,128)(2,1)S(1)} collective-permute-done((bf16[32,4096]{1,0:T(8,128)(2,1)S(1)}, bf16[32,4096]{1,0:T(8,128)(2,1)S(1)}, u32[]{:S(2)}, u32[]{:S(2)}) %collective-permute-start.15) | collective-permute-done | bytes 262176 | tf_op jit(solution)/shard_map/ppermute | solution.py:196
  55.1 2.3 %collective-permute-start.18 = (bf16[8,4096]{1,0:T(8,128)(2,1)S(1)}, bf16[8,4096]{1,0:T(8,128)(2,1)S(1)}, u32[]{:S(2)}, u32[]{:S(2)}) collective-permute-start(bf16[8,4096]{1,0:T(8,128)(2,1)S(1)} %get-tuple-element.67), channel_id=1, source_target_pairs={{0,16},{1,17},{2,18},{3,19},{4,20},{5,21},{6,22},{7,23},{8,24},{9,... | collective-permute-start | bytes 196616 | tf_op jit(solution)/shard_map/ppermute | solution.py:196
  58.5 4.3 %collective-permute-done.18 = bf16[8,4096]{1,0:T(8,128)(2,1)S(1)} collective-permute-done((bf16[8,4096]{1,0:T(8,128)(2,1)S(1)}, bf16[8,4096]{1,0:T(8,128)(2,1)S(1)}, u32[]{:S(2)}, u32[]{:S(2)}) %collective-permute-start.18) | collective-permute-done | bytes 65568 | tf_op jit(solution)/shard_map/ppermute | solution.py:196
  63.5 2.8 %collective-permute-start.24 = (bf16[8,4096]{1,0:T(8,128)(2,1)S(1)}, bf16[8,4096]{1,0:T(8,128)(2,1)S(1)}, u32[]{:S(2)}, u32[]{:S(2)}) collective-permute-start(bf16[8,4096]{1,0:T(8,128)(2,1)S(1)} %fusion.9), channel_id=1, source_target_pairs={{0,16},{1,17},{2,18},{3,19},{4,20},{5,21},{6,22},{7,23},{8,24},{9,... | collective-permute-start | bytes 196616 | tf_op jit(solution)/shard_map/ppermute | solution.py:196
  67.5 3.8 %collective-permute-done.24 = bf16[8,4096]{1,0:T(8,128)(2,1)S(1)} collective-permute-done((bf16[8,4096]{1,0:T(8,128)(2,1)S(1)}, bf16[8,4096]{1,0:T(8,128)(2,1)S(1)}, u32[]{:S(2)}, u32[]{:S(2)}) %collective-permute-start.24) | collective-permute-done | bytes 65568 | tf_op jit(solution)/shard_map/ppermute | solution.py:196
  72.6 1.6 %collective-permute-start.26 = (bf16[16,4096]{1,0:T(8,128)(2,1)S(1)}, bf16[16,4096]{1,0:T(8,128)(2,1)S(1)}, u32[]{:S(2)}, u32[]{:S(2)}) collective-permute-start(bf16[16,4096]{1,0:T(8,128)(2,1)S(1)} %constant_dynamic-update-slice_fusion.4.refs_4_), channel_id=1, source_target_pairs={{0,6},{1,7},{2,4},{3,5},{4,2},{5,3},{6,0},{7,1},{8,14},{9,15},{10,... | collective-permute-start | bytes 393224 | tf_op jit(solution)/shard_map/ppermute | solution.py:196
  74.7 1.4 %collective-permute-start.28 = (bf16[16,4096]{1,0:T(8,128)(2,1)S(1)}, bf16[16,4096]{1,0:T(8,128)(2,1)S(1)}, u32[]{:S(2)}, u32[]{:S(2)}) collective-permute-start(bf16[16,4096]{1,0:T(8,128)(2,1)S(1)} %constant_dynamic-update-slice_fusion.4.refs_4_), channel_id=1, source_target_pairs={{0,4},{1,5},{2,6},{3,7},{4,0},{5,1},{6,2},{7,3},{8,12},{9,13},{10,... | collective-permute-start | bytes 393224 | tf_op jit(solution)/shard_map/ppermute | solution.py:196
  76.1 1.6 %collective-permute-start.21 = (bf16[16,4096]{1,0:T(8,128)(2,1)S(1)}, bf16[16,4096]{1,0:T(8,128)(2,1)S(1)}, u32[]{:S(2)}, u32[]{:S(2)}) collective-permute-start(bf16[16,4096]{1,0:T(8,128)(2,1)S(1)} %pad_maximum_fusion.6.refs_0_), channel_id=1, source_target_pairs={{0,6},{1,7},{2,4},{3,5},{4,2},{5,3},{6,0},{7,1},{8,14},{9,15},{10,... | collective-permute-start | bytes 393224 | tf_op jit(solution)/shard_map/ppermute | solution.py:196
  78.3 1.7 %collective-permute-done.26.refs_5_ = bf16[16,4096]{1,0:T(8,128)(2,1)S(1)} collective-permute-done((bf16[16,4096]{1,0:T(8,128)(2,1)S(1)}, bf16[16,4096]{1,0:T(8,128)(2,1)S(1)}, u32[]{:S(2)}, u32[]{:S(2)}) %collective-permute-start.26) | collective-permute-done | bytes 131104 | tf_op jit(solution)/shard_map/ppermute | solution.py:196
  86.4 2.8 %shard_map.143.refs_16_.rows_ref = f32[256,4096]{1,0:T(8,128)S(1)} custom-call(s32[2]{0:T(128)S(1)} %pad_add_fusion.place_ref, f32[2,1,256,4096]{3,2,1,0:T(8,128)} %refs_0_.3), custom_call_target="tpu_custom_call" | custom-call | tf_op jit(solution)/shard_map/pallas_call | solution.py:255
  89.3 4.9 %shard_map.144 = (bf16[256,64]{1,0:T(8,128)(2,1)S(1)}, f32[256,512]{1,0:T(8,128)S(1)}) custom-call(s32[2]{0:T(128)S(1)} %pad_add_fusion.place_ref, bf16[16,4096]{1,0:T(8,128)(2,1)S(1)} %pad_maximum_fusion.6.refs_0_, bf16[16,4096]{1,0:T(8,128)(2,1)S(1)} %collective-permute-done.21.refs_1_, bf16[16,4096]{1,0:T(8,128)(2,1)S(1)} %collective-permute-done.22.refs_2_, ...), custom_call_target="tpu_custom_call" | custom-call | tf_op jit(solution)/shard_map/pallas_call | solution.py:357
  96.5 1.6 %collective-permute-start.33 = (bf16[32,4096]{1,0:T(8,128)(2,1)S(1)}, bf16[32,4096]{1,0:T(8,128)(2,1)S(1)}, u32[]{:S(2)}, u32[]{:S(2)}) collective-permute-start(bf16[32,4096]{1,0:T(8,128)(2,1)S(1)} %get-tuple-element.58), channel_id=1, source_target_pairs={{0,6},{1,7},{2,4},{3,5},{4,2},{5,3},{6,0},{7,1},{8,14},{9,15},{10,... | collective-permute-start | bytes 786440 | tf_op jit(solution)/shard_map/ppermute | solution.py:196
  98.6 1.4 %collective-permute-start.35 = (bf16[32,4096]{1,0:T(8,128)(2,1)S(1)}, bf16[32,4096]{1,0:T(8,128)(2,1)S(1)}, u32[]{:S(2)}, u32[]{:S(2)}) collective-permute-start(bf16[32,4096]{1,0:T(8,128)(2,1)S(1)} %get-tuple-element.56), channel_id=1, source_target_pairs={{0,4},{1,5},{2,6},{3,7},{4,0},{5,1},{6,2},{7,3},{8,12},{9,13},{10,... | collective-permute-start | bytes 786440 | tf_op jit(solution)/shard_map/ppermute | solution.py:196
  100.1 3.6 %shard_map.145 = f32[2,1,256,4096]{3,2,1,0:T(8,128)} custom-call(s32[2]{0:T(128)S(1)} %pad_add_fusion.place_ref, f32[256,512]{1,0:T(8,128)S(1)} %get-tuple-element.46.vec_ref, f32[256,4096]{1,0:T(8,128)S(1)} %shard_map.143.refs_16_.rows_ref, f32[2,1,256,4096]{3,2,1,0:T(8,128)} %shard_map.142.refs_0_), custom_call_target="tpu_custom_call", output_to_operand_aliasing={{}: (3, {})} | custom-call | tf_op jit(solution)/shard_map/pallas_call | solution.py:416
  103.7 3.0 %collective-permute-done.33 = bf16[32,4096]{1,0:T(8,128)(2,1)S(1)} collective-permute-done((bf16[32,4096]{1,0:T(8,128)(2,1)S(1)}, bf16[32,4096]{1,0:T(8,128)(2,1)S(1)}, u32[]{:S(2)}, u32[]{:S(2)}) %collective-permute-start.33) | collective-permute-done | bytes 262176 | tf_op jit(solution)/shard_map/ppermute | solution.py:196
  106.7 3.9 %collective-permute-done.34 = bf16[32,4096]{1,0:T(8,128)(2,1)S(1)} collective-permute-done((bf16[32,4096]{1,0:T(8,128)(2,1)S(1)}, bf16[32,4096]{1,0:T(8,128)(2,1)S(1)}, u32[]{:S(2)}, u32[]{:S(2)}) %collective-permute-start.34) | collective-permute-done | bytes 262176 | tf_op jit(solution)/shard_map/ppermute | solution.py:196
  113.6 2.5 %collective-permute-start.38 = (bf16[8,4096]{1,0:T(8,128)(2,1)S(1)}, bf16[8,4096]{1,0:T(8,128)(2,1)S(1)}, u32[]{:S(2)}, u32[]{:S(2)}) collective-permute-start(bf16[8,4096]{1,0:T(8,128)(2,1)S(1)} %get-tuple-element.63), channel_id=1, source_target_pairs={{0,24},{1,25},{2,26},{3,27},{4,28},{5,29},{6,30},{7,31},{8,16},{9,... | collective-permute-start | bytes 196616 | tf_op jit(solution)/shard_map/ppermute | solution.py:196
  116.7 3.9 %collective-permute-done.37 = bf16[8,4096]{1,0:T(8,128)(2,1)S(1)} collective-permute-done((bf16[8,4096]{1,0:T(8,128)(2,1)S(1)}, bf16[8,4096]{1,0:T(8,128)(2,1)S(1)}, u32[]{:S(2)}, u32[]{:S(2)}) %collective-permute-start.37) | collective-permute-done | bytes 65568 | tf_op jit(solution)/shard_map/ppermute | solution.py:196
  (86 shorter events, 32.3 us)
Async XLA Ops:
  0.7 8.0 %collective-permute-start.4 = (bf16[8,4096]{1,0:T(8,128)(2,1)}, bf16[8,4096]{1,0:T(8,128)(2,1)S(1)}, u32[]{:S(2)}, u32[]{:S(2)}) collective-permute-start(bf16[8,4096]{1,0:T(8,128)(2,1)} %bitcast.33), channel_id=1, source_target_pairs={{0,16},{1,17},{2,18},{3,19},{4,20},{5,21},{6,22},{7,23},{8,24},{9,... | collective-permute-start | bytes 196616 | tf_op jit(solution)/shard_map/ppermute | solution.py:196
  4.8 6.4 %collective-permute-start.5 = (bf16[8,4096]{1,0:T(8,128)(2,1)}, bf16[8,4096]{1,0:T(8,128)(2,1)S(1)}, u32[]{:S(2)}, u32[]{:S(2)}) collective-permute-start(bf16[8,4096]{1,0:T(8,128)(2,1)} %bitcast.34), channel_id=1, source_target_pairs={{0,24},{1,25},{2,26},{3,27},{4,28},{5,29},{6,30},{7,31},{8,16},{9,... | collective-permute-start | bytes 196616 | tf_op jit(solution)/shard_map/ppermute | solution.py:196
  6.2 8.5 %collective-permute-start = (bf16[8,4096]{1,0:T(8,128)(2,1)}, bf16[8,4096]{1,0:T(8,128)(2,1)S(1)}, u32[]{:S(2)}, u32[]{:S(2)}) collective-permute-start(bf16[8,4096]{1,0:T(8,128)(2,1)} %bitcast.35), channel_id=1, source_target_pairs={{0,8},{1,9},{2,10},{3,11},{4,12},{5,13},{6,14},{7,15},{8,0},{9,1},... | collective-permute-start | bytes 196616 | tf_op jit(solution)/shard_map/ppermute | solution.py:196
  6.4 31.5 %collective-permute-start.13 = (bf16[2,64,4096]{2,1,0:T(8,128)(2,1)}, bf16[2,64,4096]{2,1,0:T(8,128)(2,1)S(1)}, u32[]{:S(2)}, u32[]{:S(2)}) collective-permute-start(bf16[2,64,4096]{2,1,0:T(8,128)(2,1)} %bitcast.32), channel_id=1, source_target_pairs={{0,1},{1,0},{2,3},{3,2},{4,5},{5,4},{6,7},{7,6},{8,9},{9,8},{10,11... | collective-permute-start | bytes 3145736 | tf_op jit(solution)/shard_map/ppermute | solution.py:196
  11.2 7.4 %collective-permute-start.6 = (bf16[16,4096]{1,0:T(8,128)(2,1)S(1)}, bf16[16,4096]{1,0:T(8,128)(2,1)S(1)}, u32[]{:S(2)}, u32[]{:S(2)}) collective-permute-start(bf16[16,4096]{1,0:T(8,128)(2,1)S(1)} %constant_dynamic-update-slice_fusion.2.refs_4_), channel_id=1, source_target_pairs={{0,6},{1,7},{2,4},{3,5},{4,2},{5,3},{6,0},{7,1},{8,14},{9,15},{10,... | collective-permute-start | bytes 393224 | tf_op jit(solution)/shard_map/ppermute | solution.py:196
  13.6 7.7 %collective-permute-start.7 = (bf16[16,4096]{1,0:T(8,128)(2,1)S(1)}, bf16[16,4096]{1,0:T(8,128)(2,1)S(1)}, u32[]{:S(2)}, u32[]{:S(2)}) collective-permute-start(bf16[16,4096]{1,0:T(8,128)(2,1)S(1)} %constant_dynamic-update-slice_fusion.2.refs_4_), channel_id=1, source_target_pairs={{0,2},{1,3},{2,0},{3,1},{4,6},{5,7},{6,4},{7,5},{8,10},{9,11},{10,... | collective-permute-start | bytes 393224 | tf_op jit(solution)/shard_map/ppermute | solution.py:196
  14.2 7.7 %collective-permute-start.8 = (bf16[16,4096]{1,0:T(8,128)(2,1)S(1)}, bf16[16,4096]{1,0:T(8,128)(2,1)S(1)}, u32[]{:S(2)}, u32[]{:S(2)}) collective-permute-start(bf16[16,4096]{1,0:T(8,128)(2,1)S(1)} %constant_dynamic-update-slice_fusion.2.refs_4_), channel_id=1, source_target_pairs={{0,4},{1,5},{2,6},{3,7},{4,0},{5,1},{6,2},{7,3},{8,12},{9,13},{10,... | collective-permute-start | bytes 393224 | tf_op jit(solution)/shard_map/ppermute | solution.py:196
  14.7 8.3 %collective-permute-start.1 = (bf16[16,4096]{1,0:T(8,128)(2,1)S(1)}, bf16[16,4096]{1,0:T(8,128)(2,1)S(1)}, u32[]{:S(2)}, u32[]{:S(2)}) collective-permute-start(bf16[16,4096]{1,0:T(8,128)(2,1)S(1)} %constant_dynamic-update-slice_fusion.refs_0_), channel_id=1, source_target_pairs={{0,6},{1,7},{2,4},{3,5},{4,2},{5,3},{6,0},{7,1},{8,14},{9,15},{10,... | collective-permute-start | bytes 393224 | tf_op jit(solution)/shard_map/ppermute | solution.py:196
  18.6 5.8 %collective-permute-start.2 = (bf16[16,4096]{1,0:T(8,128)(2,1)S(1)}, bf16[16,4096]{1,0:T(8,128)(2,1)S(1)}, u32[]{:S(2)}, u32[]{:S(2)}) collective-permute-start(bf16[16,4096]{1,0:T(8,128)(2,1)S(1)} %constant_dynamic-update-slice_fusion.refs_0_), channel_id=1, source_target_pairs={{0,2},{1,3},{2,0},{3,1},{4,6},{5,7},{6,4},{7,5},{8,10},{9,11},{10,... | collective-permute-start | bytes 393224 | tf_op jit(solution)/shard_map/ppermute | solution.py:196
  21.9 9.9 %collective-permute-start.11 = (bf16[48,4096]{1,0:T(8,128)(2,1)S(1)}, bf16[48,4096]{1,0:T(8,128)(2,1)S(1)}, u32[]{:S(2)}, u32[]{:S(2)}) collective-permute-start(bf16[48,4096]{1,0:T(8,128)(2,1)S(1)} %pad_maximum_fusion.1), channel_id=1, source_target_pairs={{0,1},{1,0},{2,3},{3,2},{4,5},{5,4},{6,7},{7,6},{8,9},{9,8},{10,11... | collective-permute-start | bytes 1179656 | tf_op jit(solution)/shard_map/ppermute | solution.py:196
  26.4 5.5 %collective-permute-start.10 = (bf16[48,4096]{1,0:T(8,128)(2,1)S(1)}, bf16[48,4096]{1,0:T(8,128)(2,1)S(1)}, u32[]{:S(2)}, u32[]{:S(2)}) collective-permute-start(bf16[48,4096]{1,0:T(8,128)(2,1)S(1)} %pad_maximum_fusion), channel_id=1, source_target_pairs={{0,1},{1,0},{2,3},{3,2},{4,5},{5,4},{6,7},{7,6},{8,9},{9,8},{10,11... | collective-permute-start | bytes 1179656 | tf_op jit(solution)/shard_map/ppermute | solution.py:196
  26.5 5.3 %collective-permute-start.9 = (bf16[32,4096]{1,0:T(8,128)(2,1)S(1)}, bf16[32,4096]{1,0:T(8,128)(2,1)S(1)}, u32[]{:S(2)}, u32[]{:S(2)}) collective-permute-start(bf16[32,4096]{1,0:T(8,128)(2,1)S(1)} %pad_maximum_fusion.4), channel_id=1, source_target_pairs={{0,1},{1,0},{2,3},{3,2},{4,5},{5,4},{6,7},{7,6},{8,9},{9,8},{10,11... | collective-permute-start | bytes 786440 | tf_op jit(solution)/shard_map/ppermute | solution.py:196
  38.9 10.2 %collective-permute-start.14 = (bf16[32,4096]{1,0:T(8,128)(2,1)S(1)}, bf16[32,4096]{1,0:T(8,128)(2,1)S(1)}, u32[]{:S(2)}, u32[]{:S(2)}) collective-permute-start(bf16[32,4096]{1,0:T(8,128)(2,1)S(1)} %get-tuple-element.61), channel_id=1, source_target_pairs={{0,6},{1,7},{2,4},{3,5},{4,2},{5,3},{6,0},{7,1},{8,14},{9,15},{10,... | collective-permute-start | bytes 786440 | tf_op jit(solution)/shard_map/ppermute | solution.py:196
  40.5 12.5 %collective-permute-start.15 = (bf16[32,4096]{1,0:T(8,128)(2,1)S(1)}, bf16[32,4096]{1,0:T(8,128)(2,1)S(1)}, u32[]{:S(2)}, u32[]{:S(2)}) collective-permute-start(bf16[32,4096]{1,0:T(8,128)(2,1)S(1)} %get-tuple-element.60), channel_id=1, source_target_pairs={{0,2},{1,3},{2,0},{3,1},{4,6},{5,7},{6,4},{7,5},{8,10},{9,11},{10,... | collective-permute-start | bytes 786440 | tf_op jit(solution)/shard_map/ppermute | solution.py:196
  41.0 12.9 %collective-permute-start.16 = (bf16[32,4096]{1,0:T(8,128)(2,1)S(1)}, bf16[32,4096]{1,0:T(8,128)(2,1)S(1)}, u32[]{:S(2)}, u32[]{:S(2)}) collective-permute-start(bf16[32,4096]{1,0:T(8,128)(2,1)S(1)} %get-tuple-element.59), channel_id=1, source_target_pairs={{0,4},{1,5},{2,6},{3,7},{4,0},{5,1},{6,2},{7,3},{8,12},{9,13},{10,... | collective-permute-start | bytes 786440 | tf_op jit(solution)/shard_map/ppermute | solution.py:196
  55.1 7.7 %collective-permute-start.18 = (bf16[8,4096]{1,0:T(8,128)(2,1)S(1)}, bf16[8,4096]{1,0:T(8,128)(2,1)S(1)}, u32[]{:S(2)}, u32[]{:S(2)}) collective-permute-start(bf16[8,4096]{1,0:T(8,128)(2,1)S(1)} %get-tuple-element.67), channel_id=1, source_target_pairs={{0,16},{1,17},{2,18},{3,19},{4,20},{5,21},{6,22},{7,23},{8,24},{9,... | collective-permute-start | bytes 196616 | tf_op jit(solution)/shard_map/ppermute | solution.py:196
  57.4 6.1 %collective-permute-start.19 = (bf16[8,4096]{1,0:T(8,128)(2,1)S(1)}, bf16[8,4096]{1,0:T(8,128)(2,1)S(1)}, u32[]{:S(2)}, u32[]{:S(2)}) collective-permute-start(bf16[8,4096]{1,0:T(8,128)(2,1)S(1)} %get-tuple-element.66), channel_id=1, source_target_pairs={{0,24},{1,25},{2,26},{3,27},{4,28},{5,29},{6,30},{7,31},{8,16},{9,... | collective-permute-start | bytes 196616 | tf_op jit(solution)/shard_map/ppermute | solution.py:196
  63.5 7.8 %collective-permute-start.24 = (bf16[8,4096]{1,0:T(8,128)(2,1)S(1)}, bf16[8,4096]{1,0:T(8,128)(2,1)S(1)}, u32[]{:S(2)}, u32[]{:S(2)}) collective-permute-start(bf16[8,4096]{1,0:T(8,128)(2,1)S(1)} %fusion.9), channel_id=1, source_target_pairs={{0,16},{1,17},{2,18},{3,19},{4,20},{5,21},{6,22},{7,23},{8,24},{9,... | collective-permute-start | bytes 196616 | tf_op jit(solution)/shard_map/ppermute | solution.py:196
  66.4 6.2 %collective-permute-start.25 = (bf16[8,4096]{1,0:T(8,128)(2,1)S(1)}, bf16[8,4096]{1,0:T(8,128)(2,1)S(1)}, u32[]{:S(2)}, u32[]{:S(2)}) collective-permute-start(bf16[8,4096]{1,0:T(8,128)(2,1)S(1)} %fusion.9), channel_id=1, source_target_pairs={{0,24},{1,25},{2,26},{3,27},{4,28},{5,29},{6,30},{7,31},{8,16},{9,... | collective-permute-start | bytes 196616 | tf_op jit(solution)/shard_map/ppermute | solution.py:196
  67.5 8.5 %collective-permute-start.20 = (bf16[8,4096]{1,0:T(8,128)(2,1)S(1)}, bf16[8,4096]{1,0:T(8,128)(2,1)S(1)}, u32[]{:S(2)}, u32[]{:S(2)}) collective-permute-start(bf16[8,4096]{1,0:T(8,128)(2,1)S(1)} %fusion.9), channel_id=1, source_target_pairs={{0,8},{1,9},{2,10},{3,11},{4,12},{5,13},{6,14},{7,15},{8,0},{9,1},... | collective-permute-start | bytes 196616 | tf_op jit(solution)/shard_map/ppermute | solution.py:196
  72.6 7.4 %collective-permute-start.26 = (bf16[16,4096]{1,0:T(8,128)(2,1)S(1)}, bf16[16,4096]{1,0:T(8,128)(2,1)S(1)}, u32[]{:S(2)}, u32[]{:S(2)}) collective-permute-start(bf16[16,4096]{1,0:T(8,128)(2,1)S(1)} %constant_dynamic-update-slice_fusion.4.refs_4_), channel_id=1, source_target_pairs={{0,6},{1,7},{2,4},{3,5},{4,2},{5,3},{6,0},{7,1},{8,14},{9,15},{10,... | collective-permute-start | bytes 393224 | tf_op jit(solution)/shard_map/ppermute | solution.py:196
  74.2 7.7 %collective-permute-start.27 = (bf16[16,4096]{1,0:T(8,128)(2,1)S(1)}, bf16[16,4096]{1,0:T(8,128)(2,1)S(1)}, u32[]{:S(2)}, u32[]{:S(2)}) collective-permute-start(bf16[16,4096]{1,0:T(8,128)(2,1)S(1)} %constant_dynamic-update-slice_fusion.4.refs_4_), channel_id=1, source_target_pairs={{0,2},{1,3},{2,0},{3,1},{4,6},{5,7},{6,4},{7,5},{8,10},{9,11},{10,... | collective-permute-start | bytes 393224 | tf_op jit(solution)/shard_map/ppermute | solution.py:196
  74.7 8.5 %collective-permute-start.28 = (bf16[16,4096]{1,0:T(8,128)(2,1)S(1)}, bf16[16,4096]{1,0:T(8,128)(2,1)S(1)}, u32[]{:S(2)}, u32[]{:S(2)}) collective-permute-start(bf16[16,4096]{1,0:T(8,128)(2,1)S(1)} %constant_dynamic-update-slice_fusion.4.refs_4_), channel_id=1, source_target_pairs={{0,4},{1,5},{2,6},{3,7},{4,0},{5,1},{6,2},{7,3},{8,12},{9,13},{10,... | collective-permute-start | bytes 393224 | tf_op jit(solution)/shard_map/ppermute | solution.py:196
  76.1 8.3 %collective-permute-start.21 = (bf16[16,4096]{1,0:T(8,128)(2,1)S(1)}, bf16[16,4096]{1,0:T(8,128)(2,1)S(1)}, u32[]{:S(2)}, u32[]{:S(2)}) collective-permute-start(bf16[16,4096]{1,0:T(8,128)(2,1)S(1)} %pad_maximum_fusion.6.refs_0_), channel_id=1, source_target_pairs={{0,6},{1,7},{2,4},{3,5},{4,2},{5,3},{6,0},{7,1},{8,14},{9,15},{10,... | collective-permute-start | bytes 393224 | tf_op jit(solution)/shard_map/ppermute | solution.py:196
  77.7 7.1 %collective-permute-start.22 = (bf16[16,4096]{1,0:T(8,128)(2,1)S(1)}, bf16[16,4096]{1,0:T(8,128)(2,1)S(1)}, u32[]{:S(2)}, u32[]{:S(2)}) collective-permute-start(bf16[16,4096]{1,0:T(8,128)(2,1)S(1)} %pad_maximum_fusion.6.refs_0_), channel_id=1, source_target_pairs={{0,2},{1,3},{2,0},{3,1},{4,6},{5,7},{6,4},{7,5},{8,10},{9,11},{10,... | collective-permute-start | bytes 393224 | tf_op jit(solution)/shard_map/ppermute | solution.py:196
  79.9 5.8 %collective-permute-start.23 = (bf16[16,4096]{1,0:T(8,128)(2,1)S(1)}, bf16[16,4096]{1,0:T(8,128)(2,1)S(1)}, u32[]{:S(2)}, u32[]{:S(2)}) collective-permute-start(bf16[16,4096]{1,0:T(8,128)(2,1)S(1)} %pad_maximum_fusion.6.refs_0_), channel_id=1, source_target_pairs={{0,4},{1,5},{2,6},{3,7},{4,0},{5,1},{6,2},{7,3},{8,12},{9,13},{10,... | collective-permute-start | bytes 393224 | tf_op jit(solution)/shard_map/ppermute | solution.py:196
  83.2 6.1 %collective-permute-start.31 = (bf16[48,4096]{1,0:T(8,128)(2,1)S(1)}, bf16[48,4096]{1,0:T(8,128)(2,1)S(1)}, u32[]{:S(2)}, u32[]{:S(2)}) collective-permute-start(bf16[48,4096]{1,0:T(8,128)(2,1)S(1)} %pad_maximum_fusion.3), channel_id=1, source_target_pairs={{0,1},{1,0},{2,3},{3,2},{4,5},{5,4},{6,7},{7,6},{8,9},{9,8},{10,11... | collective-permute-start | bytes 1179656 | tf_op jit(solution)/shard_map/ppermute | solution.py:196
  96.5 10.2 %collective-permute-start.33 = (bf16[32,4096]{1,0:T(8,128)(2,1)S(1)}, bf16[32,4096]{1,0:T(8,128)(2,1)S(1)}, u32[]{:S(2)}, u32[]{:S(2)}) collective-permute-start(bf16[32,4096]{1,0:T(8,128)(2,1)S(1)} %get-tuple-element.58), channel_id=1, source_target_pairs={{0,6},{1,7},{2,4},{3,5},{4,2},{5,3},{6,0},{7,1},{8,14},{9,15},{10,... | collective-permute-start | bytes 786440 | tf_op jit(solution)/shard_map/ppermute | solution.py:196
  98.1 12.5 %collective-permute-start.34 = (bf16[32,4096]{1,0:T(8,128)(2,1)S(1)}, bf16[32,4096]{1,0:T(8,128)(2,1)S(1)}, u32[]{:S(2)}, u32[]{:S(2)}) collective-permute-start(bf16[32,4096]{1,0:T(8,128)(2,1)S(1)} %get-tuple-element.57), channel_id=1, source_target_pairs={{0,2},{1,3},{2,0},{3,1},{4,6},{5,7},{6,4},{7,5},{8,10},{9,11},{10,... | collective-permute-start | bytes 786440 | tf_op jit(solution)/shard_map/ppermute | solution.py:196
  98.6 12.8 %collective-permute-start.35 = (bf16[32,4096]{1,0:T(8,128)(2,1)S(1)}, bf16[32,4096]{1,0:T(8,128)(2,1)S(1)}, u32[]{:S(2)}, u32[]{:S(2)}) collective-permute-start(bf16[32,4096]{1,0:T(8,128)(2,1)S(1)} %get-tuple-element.56), channel_id=1, source_target_pairs={{0,4},{1,5},{2,6},{3,7},{4,0},{5,1},{6,2},{7,3},{8,12},{9,13},{10,... | collective-permute-start | bytes 786440 | tf_op jit(solution)/shard_map/ppermute | solution.py:196
  112.4 8.1 %collective-permute-start.37 = (bf16[8,4096]{1,0:T(8,128)(2,1)S(1)}, bf16[8,4096]{1,0:T(8,128)(2,1)S(1)}, u32[]{:S(2)}, u32[]{:S(2)}) collective-permute-start(bf16[8,4096]{1,0:T(8,128)(2,1)S(1)} %get-tuple-element.64), channel_id=1, source_target_pairs={{0,16},{1,17},{2,18},{3,19},{4,20},{5,21},{6,22},{7,23},{8,24},{9,... | collective-permute-start | bytes 196616 | tf_op jit(solution)/shard_map/ppermute | solution.py:196
  113.6 6.9 %collective-permute-start.38 = (bf16[8,4096]{1,0:T(8,128)(2,1)S(1)}, bf16[8,4096]{1,0:T(8,128)(2,1)S(1)}, u32[]{:S(2)}, u32[]{:S(2)}) collective-permute-start(bf16[8,4096]{1,0:T(8,128)(2,1)S(1)} %get-tuple-element.63), channel_id=1, source_target_pairs={{0,24},{1,25},{2,26},{3,27},{4,28},{5,29},{6,30},{7,31},{8,16},{9,... | collective-permute-start | bytes 196616 | tf_op jit(solution)/shard_map/ppermute | solution.py:196
  (9 other events, 51.4 us)
where the time goes:
time: 121 us
  waiting for transfers between devices  50 us (41%)
  starting transfers between devices  41.6 us (34%)
  Pallas kernels  24.5 us (20%)
  matrix products  1.67 us (1%)
  other arithmetic  1.44 us (1%)
    ppermute x39, waiting for transfers between devices, moved(): lax.ppermute(part, 'tp', [(i, i ^ mask) for i in range(lax.axis_size('tp'...  50 us
    ppermute x39, starting transfers between devices, moved(): lax.ppermute(part, 'tp', [(i, i ^ mask) for i in range(lax.axis_size('tp'...  41.6 us
    pallas_call x2, Pallas kernels, front(): pl.pallas_call(partial(front_kernel, piece_rows=piece_rows, head_size=hea...  9.67 us
    pallas_call x2, Pallas kernels, load(): pl.pallas_call(partial(load_kernel, layer=layer, layers=layers, count=len...  7.57 us
    pallas_call x2, Pallas kernels, update(): pl.pallas_call(partial(update_kernel, seq_tile=seqs // lax.axis_size('tp'...  7.24 us
  transfers between devices with their start and end apart: 39, of which 27 were waited for; matrix products, arithmetic and copies ran while one was open for 1% of the time, Pallas kernels for 16%

commit v1 on v0

--- a/solution.py
+++ b/solution.py
@@ -371,7 +371,7 @@
     )(place, *[near(piece) for piece in pieces], near(gain), *[near(t) for t in tables], near(packed), near(rows))
 
 
-def update_kernel(place_ref, vec_ref, rows_ref, *refs, seq_tile, head_size, layer):
+def update_kernel(place_ref, vec_ref, rows_ref, *refs, seq_tile, head_size, layer, part):
     out_ref, spread_ref, results_ref, written = refs[-4:]
     wide = 2 * head_size
     seqs, columns = rows_ref.shape
@@ -381,8 +381,13 @@
     spread_ref[...] = jnp.where(at_row == at_lane, 1.0, 0.0).astype(jnp.bfloat16)
     tiles = list(slots(place_ref, seqs, seq_tile))
     per_block = STATE_ROWS // seq_tile
-    for block in range(seqs // STATE_ROWS):
+    blocks = seqs // STATE_ROWS // CORES
+    blocks = range(part * blocks, (part + 1) * blocks)
+    for block in blocks:
         span = slice(block * STATE_ROWS, (block + 1) * STATE_ROWS)
+        local = slice(
+            (block - blocks[0]) * STATE_ROWS, (block - blocks[0] + 1) * STATE_ROWS
+        )
         pair = vec_ref[span, 3 * wide :]
         high = pair.astype(jnp.bfloat16)
         low = (pair - high.astype(jnp.float32)).astype(jnp.bfloat16)
@@ -393,21 +398,22 @@
             return jnp.dot(both, spread_ref[...], preferred_element_type=jnp.float32)
 
         row = lambda at: jnp.tile(vec_ref[span, at * wide : (at + 1) * wide], (1, repeats))
-        results_ref[span, :] = rows_ref[span, :] * row(0) - spread(1) * row(1) + spread(0) * row(2)
+        results_ref[local, :] = rows_ref[span, :] * row(0) - spread(1) * row(1) + spread(0) * row(2)
         for slot in range(block * per_block, (block + 1) * per_block):
+            at = slot * seq_tile - blocks[0] * STATE_ROWS
             pltpu.make_async_copy(
-                results_ref.at[slot * seq_tile : (slot + 1) * seq_tile],
+                results_ref.at[at : at + seq_tile],
                 out_ref.at[layer, 0, pl.ds(tiles[slot], seq_tile)],
-                written.at[block],
+                written.at[block - blocks[0]],
             ).start()
-    for block in range(seqs // STATE_ROWS):
-        span = slice(block * STATE_ROWS, (block + 1) * STATE_ROWS)
+    for at in range(len(blocks)):
+        span = slice(at * STATE_ROWS, (at + 1) * STATE_ROWS)
         pltpu.make_async_copy(
-            results_ref.at[span], out_ref.at[layer, 0, :STATE_ROWS], written.at[block]
+            results_ref.at[span], out_ref.at[layer, 0, :STATE_ROWS], written.at[at]
         ).wait()
 
 
-def update(place, vec, rows, previous, shape, layer):
+def update(place, vec, rows, previous, shape, layer, part):
     seqs, columns = rows.shape
     head_size = vec.shape[1] // 8
     vmem = pl.BlockSpec(memory_space=pltpu.VMEM)
@@ -419,13 +425,14 @@
             seq_tile=seqs // lax.axis_size("tp"),
             head_size=head_size,
             layer=layer,
+            part=part,
         ),
         in_specs=[pl.BlockSpec(memory_space=pltpu.SMEM), vmem, vmem] + [hbm] * len(more),
         out_specs=hbm,
         scratch_shapes=[
             pltpu.VMEM((2 * head_size, columns), jnp.bfloat16),
-            pltpu.VMEM((seqs, columns), jnp.float32),
-            pltpu.SemaphoreType.DMA((seqs // STATE_ROWS,)),
+            pltpu.VMEM((seqs // CORES, columns), jnp.float32),
+            pltpu.SemaphoreType.DMA((seqs // STATE_ROWS // CORES,)),
         ],
         out_shape=jax.ShapeDtypeStruct(shape, rows.dtype),
         input_output_aliases={3: 0} if more else {},
@@ -435,41 +442,38 @@
 
 def gather_tiles(tile, levels):
     step = CORES * PLANE
-    groups = [jnp.concatenate([tile, moved(tile, step)], 0)]
-    if levels > 2:
-        distant = [moved(tile, step * apart) for apart in range(2, levels)]
-        groups.append(jnp.concatenate(distant, 0))
-    rows = tile.shape[0]
-    half = PLANE * levels * rows
-    part = lambda q, at, size: [q * levels * rows + at + r for r in range(0, size, 16)]
-    pieces, places, swaps = [], [], []
-    start = 0
-    for group in groups:
-        order = (3, 1, 2)
-        got = [moved(group, CORES * q) for q in order]
-        pieces += [group] + got
-        places += [part(q, start, group.shape[0]) for q in (0, *order)]
-        swaps.append((got, [r for q in order for r in part(q, start, group.shape[0])]))
-        start += group.shape[0]
-    swaps.insert(0, (groups, part(0, 0, start)))
-    for parts, spots in swaps:
-        pieces.append(moved(jnp.concatenate(parts, 0), 1))
-        places.append([half + r for r in spots])
+    corner = moved(tile, CORES * 3)
+    column = {at: moved(tile, step * at) for at in range(1, levels)}
+    corners = {at: moved(corner, step * at) for at in range(1, levels)}
+    column = jnp.concatenate([tile, *column.values()], 0)
+    across = [moved(column, CORES * q) for q in (1, 2)]
+    corners = jnp.concatenate([corner, *corners.values()], 0)
+    pieces = [column, *across, corners]
+    pieces += [moved(piece, 1) for piece in pieces]
+    block = column.shape[0]
+    places = [[at * block + r for r in range(0, block, 16)] for at in range(len(pieces))]
     return pieces, places
 
 
-def sum_tiles(parts, levels, during):
+def sum_tiles(parts, levels, new_state, update_part):
     rows = parts.shape[0] // (PLANE * levels)
     block = levels * rows
+    step = CORES * PLANE
+    wide = lambda got: [part.astype(jnp.float32) for part in got]
     sends = parts.astype(jnp.bfloat16)
-    got = [moved(sends[q * block : (q + 1) * block], CORES * q) for q in (3, 1, 2)]
-    *got, during = lax.optimization_barrier((*got, during))
-    summed = parts[:block] + sum(part.astype(jnp.float32) for part in got)
+    across = [moved(sends[q * block : (q + 1) * block], CORES * q) for q in (1, 2)]
+    diagonal = sends[3 * block :]
+    along = [moved(diagonal[at * rows : (at + 1) * rows], step * at) for at in range(1, levels)]
+    new_state = update_part(new_state, 0)
+    *across, new_state = lax.optimization_barrier((*across, new_state))
+    summed = parts[:block] + sum(wide(across))
     sends = summed.astype(jnp.bfloat16)
-    got = [
-        moved(sends[at * rows : (at + 1) * rows], CORES * PLANE * at) for at in range(1, levels)
-    ]
-    return summed[:rows] + sum(part.astype(jnp.float32) for part in got), during
+    got = [moved(sends[at * rows : (at + 1) * rows], step * at) for at in range(1, levels)]
+    corner = (parts[3 * block : 3 * block + rows] + sum(wide(along))).astype(jnp.bfloat16)
+    got.append(moved(corner, CORES * 3))
+    new_state = update_part(new_state, 1)
+    *got, new_state = lax.optimization_barrier((*got, new_state))
+    return summed[:rows] + sum(wide(got)), new_state
 
 
 def on_device_whole(
@@ -522,8 +526,10 @@
         parts = jnp.dot(out[:half], own_out[layer], preferred_element_type=jnp.float32)
         parts += jnp.dot(moved(out[half:], 1), other_out[layer], preferred_element_type=jnp.float32)
         parts, vec = lax.optimization_barrier((parts, vec))
-        new_state = update(place, vec, rows, new_state, state.shape, layer)
-        total, new_state = sum_tiles(parts, levels, new_state)
+        update_part = lambda previous, part: update(
+            place, vec, rows, previous, state.shape, layer, part
+        )
+        total, new_state = sum_tiles(parts, levels, new_state, update_part)
         tile = (tile.astype(jnp.float32) + total).astype(jnp.bfloat16)
     return (tile[None], new_state)
 

time: 121 us -> 123 us (1.017)
  waiting for transfers between devices: 50 us -> 35.2 us
  starting transfers between devices: 41.6 us -> 54.6 us
  Pallas kernels: 24.5 us -> 27.8 us
    ppermute x39 -> x47, waiting for transfers between devices: 50 us -> 35.2 us  [moved(): lax.ppermute(part, 'tp', [(i, i ^ mask) for i in range(lax.axis_size('tp'...]
    ppermute x39 -> x47, starting transfers between devices: 41.6 us -> 54.6 us  [moved(): lax.ppermute(part, 'tp', [(i, i ^ mask) for i in range(lax.axis_size('tp'...]
    pallas_call x2 -> x4, Pallas kernels: 7.24 us -> 10.6 us  [update(): pl.pallas_call(partial(update_kernel, seq_tile=seqs // lax.axis_size('tp'...]
  transfers between devices with their start and end apart: 39 -> 47, of which waited for: 27 -> 17; matrix products, arithmetic and copies ran while one was open for 1% -> 1% of each run, Pallas kernels for 16% -> 19%
where the time goes in v1:
time: 123 us
  starting transfers between devices  54.6 us (44%)
  waiting for transfers between devices  35.2 us (29%)
  Pallas kernels  27.8 us (23%)
  matrix products  1.66 us (1%)
  other arithmetic  1.33 us (1%)
    ppermute x47, starting transfers between devices, moved(): lax.ppermute(part, 'tp', [(i, i ^ mask) for i in range(lax.axis_size('tp'...  54.6 us
    ppermute x47, waiting for transfers between devices, moved(): lax.ppermute(part, 'tp', [(i, i ^ mask) for i in range(lax.axis_size('tp'...  35.2 us
    pallas_call x4, Pallas kernels, update(): pl.pallas_call(partial(update_kernel, seq_tile=seqs // lax.axis_size('tp'...  10.6 us
    pallas_call x2, Pallas kernels, front(): pl.pallas_call(partial(front_kernel, piece_rows=piece_rows, head_size=hea...  9.66 us
    pallas_call x2, Pallas kernels, load(): pl.pallas_call(partial(load_kernel, layer=layer, layers=layers, count=len...  7.57 us
  transfers between devices with their start and end apart: 47, of which 17 were waited for; matrix products, arithmetic and copies ran while one was open for 1% of the time, Pallas kernels for 19%

profile of v1, /device:TPU:0, one launch (start us, length us, event | category | flops | bytes accessed | tf_op | source)
XLA Modules:
  0.0 122.7 jit_solution(3975349614334696063)
XLA Ops:
  0.7 3.1 %collective-permute-start = (bf16[8,4096]{1,0:T(8,128)(2,1)}, bf16[8,4096]{1,0:T(8,128)(2,1)S(1)}, u32[]{:S(2)}, u32[]{:S(2)}) collective-permute-start(bf16[8,4096]{1,0:T(8,128)(2,1)} %bitcast.33), channel_id=1, source_target_pairs={{0,8},{1,9},{2,10},{3,11},{4,12},{5,13},{6,14},{7,15},{8,0},{9,1},... | collective-permute-start | bytes 196616 | tf_op jit(solution)/shard_map/ppermute | solution.py:196
  3.8 2.6 %collective-permute-start.1 = (bf16[8,4096]{1,0:T(8,128)(2,1)}, bf16[8,4096]{1,0:T(8,128)(2,1)S(1)}, u32[]{:S(2)}, u32[]{:S(2)}) collective-permute-start(bf16[8,4096]{1,0:T(8,128)(2,1)} %bitcast.34), channel_id=1, source_target_pairs={{0,16},{1,17},{2,18},{3,19},{4,20},{5,21},{6,22},{7,23},{8,24},{9,... | collective-permute-start | bytes 196616 | tf_op jit(solution)/shard_map/ppermute | solution.py:196
  6.4 2.7 %collective-permute-start.5 = (bf16[8,4096]{1,0:T(8,128)(2,1)}, bf16[8,4096]{1,0:T(8,128)(2,1)S(1)}, u32[]{:S(2)}, u32[]{:S(2)}) collective-permute-start(bf16[8,4096]{1,0:T(8,128)(2,1)} %bitcast.36), channel_id=1, source_target_pairs={{0,6},{1,7},{2,4},{3,5},{4,2},{5,3},{6,0},{7,1},{8,14},{9,15},{10,... | collective-permute-start | bytes 196616 | tf_op jit(solution)/shard_map/ppermute | solution.py:196
  15.7 4.5 %collective-permute-done.6 = bf16[8,4096]{1,0:T(8,128)(2,1)S(1)} collective-permute-done((bf16[8,4096]{1,0:T(8,128)(2,1)S(1)}, bf16[8,4096]{1,0:T(8,128)(2,1)S(1)}, u32[]{:S(2)}, u32[]{:S(2)}) %collective-permute-start.6) | collective-permute-done | bytes 65568 | tf_op jit(solution)/shard_map/ppermute | solution.py:196
  21.8 4.4 %collective-permute-done.7 = bf16[8,4096]{1,0:T(8,128)(2,1)S(1)} collective-permute-done((bf16[8,4096]{1,0:T(8,128)(2,1)S(1)}, bf16[8,4096]{1,0:T(8,128)(2,1)S(1)}, u32[]{:S(2)}, u32[]{:S(2)}) %collective-permute-start.7) | collective-permute-done | bytes 65568 | tf_op jit(solution)/shard_map/ppermute | solution.py:196
  26.2 1.8 %collective-permute-start.8 = (bf16[8,4096]{1,0:T(8,128)(2,1)S(1)}, bf16[8,4096]{1,0:T(8,128)(2,1)S(1)}, u32[]{:S(2)}, u32[]{:S(2)}) collective-permute-start(bf16[8,4096]{1,0:T(8,128)(2,1)S(1)} %collective-permute-done.5), channel_id=1, source_target_pairs={{0,24},{1,25},{2,26},{3,27},{4,28},{5,29},{6,30},{7,31},{8,16},{9,... | collective-permute-start | bytes 196616 | tf_op jit(solution)/shard_map/ppermute | solution.py:196
  28.0 4.2 %collective-permute-done.8 = bf16[8,4096]{1,0:T(8,128)(2,1)S(1)} collective-permute-done((bf16[8,4096]{1,0:T(8,128)(2,1)S(1)}, bf16[8,4096]{1,0:T(8,128)(2,1)S(1)}, u32[]{:S(2)}, u32[]{:S(2)}) %collective-permute-start.8) | collective-permute-done | bytes 65568 | tf_op jit(solution)/shard_map/ppermute | solution.py:196
  32.8 4.8 %shard_map.140 = (f32[256,4096]{1,0:T(8,128)S(1)}, bf16[384,4096]{1,0:T(8,128)(2,1)S(1)}, bf16[384,4096]{1,0:T(8,128)(2,1)S(1)}, f32[2,4096]{1,0:T(2,128)S(1)}, ...) custom-call(s32[2]{0:T(128)S(1)} %pad_add_fusion.place_ref, f32[2,1,256,4096]{3,2,1,0:T(8,128)} %refs_0_.3, ...), custom_call_target="tpu_custom_call" | custom-call | tf_op jit(solution)/shard_map/pallas_call | solution.py:255
  37.6 4.7 %shard_map.141 = (bf16[256,64]{1,0:T(8,128)(2,1)S(1)}, f32[256,512]{1,0:T(8,128)S(1)}) custom-call(s32[2]{0:T(128)S(1)} %pad_add_fusion.place_ref, bf16[32,4096]{1,0:T(8,128)(2,1)S(1)} %constant_dynamic-update-slice_fusion.refs_0_, bf16[32,4096]{1,0:T(8,128)(2,1)S(1)} %collective-permute-done.3.refs_1_, bf16[32,4096]{1,0:T(8,128)(2,1)S(1)} %collective-permute-done.4.refs_2_, ...), custom_call_target="tpu_custom_call" | custom-call | tf_op jit(solution)/shard_map/pallas_call | solution.py:357
  44.8 1.9 %collective-permute-start.22 = (bf16[8,4096]{1,0:T(8,128)(2,1)S(1)}, bf16[8,4096]{1,0:T(8,128)(2,1)S(1)}, u32[]{:S(2)}, u32[]{:S(2)}) collective-permute-start(bf16[8,4096]{1,0:T(8,128)(2,1)S(1)} %get-tuple-element.78), channel_id=1, source_target_pairs={{0,24},{1,25},{2,26},{3,27},{4,28},{5,29},{6,30},{7,31},{8,16},{9,... | collective-permute-start | bytes 196616 | tf_op jit(solution)/shard_map/ppermute | solution.py:196
  46.7 2.6 %collective-permute-start.20 = (bf16[8,4096]{1,0:T(8,128)(2,1)S(1)}, bf16[8,4096]{1,0:T(8,128)(2,1)S(1)}, u32[]{:S(2)}, u32[]{:S(2)}) collective-permute-start(bf16[8,4096]{1,0:T(8,128)(2,1)S(1)} %get-tuple-element.77), channel_id=1, source_target_pairs={{0,8},{1,9},{2,10},{3,11},{4,12},{5,13},{6,14},{7,15},{8,0},{9,1},... | collective-permute-start | bytes 196616 | tf_op jit(solution)/shard_map/ppermute | solution.py:196
  50.4 2.6 %shard_map.142.refs_0_ = f32[2,1,256,4096]{3,2,1,0:T(8,128)} custom-call(s32[2]{0:T(128)S(1)} %pad_add_fusion.place_ref, f32[256,512]{1,0:T(8,128)S(1)} %get-tuple-element.46.vec_ref, f32[256,4096]{1,0:T(8,128)S(1)} %get-tuple-element.42.refs_13_.rows_ref), custom_call_target="tpu_custom_call" | custom-call | tf_op jit(solution)/shard_map/pallas_call | solution.py:422
  55.6 2.0 %collective-permute-done.15 = bf16[32,4096]{1,0:T(8,128)(2,1)S(1)} collective-permute-done((bf16[32,4096]{1,0:T(8,128)(2,1)S(1)}, bf16[32,4096]{1,0:T(8,128)(2,1)S(1)}, u32[]{:S(2)}, u32[]{:S(2)}) %collective-permute-start.15) | collective-permute-done | bytes 262176 | tf_op jit(solution)/shard_map/ppermute | solution.py:196
  60.2 2.0 %collective-permute-start.19 = (bf16[8,4096]{1,0:T(8,128)(2,1)S(1)}, bf16[8,4096]{1,0:T(8,128)(2,1)S(1)}, u32[]{:S(2)}, u32[]{:S(2)}) collective-permute-start(bf16[8,4096]{1,0:T(8,128)(2,1)S(1)} %get-tuple-element.85), channel_id=1, source_target_pairs={{0,24},{1,25},{2,26},{3,27},{4,28},{5,29},{6,30},{7,31},{8,16},{9,... | collective-permute-start | bytes 196616 | tf_op jit(solution)/shard_map/ppermute | solution.py:196
  62.2 2.6 %shard_map.143.refs_0_ = f32[2,1,256,4096]{3,2,1,0:T(8,128)} custom-call(s32[2]{0:T(128)S(1)} %pad_add_fusion.place_ref, f32[256,512]{1,0:T(8,128)S(1)} %get-tuple-element.46.vec_ref, f32[256,4096]{1,0:T(8,128)S(1)} %get-tuple-element.42.refs_13_.rows_ref, f32[2,1,256,4096]{3,2,1,0:T(8,128)} %shard_map.142.refs_0_), custom_call_target="tpu_custom_call", output_to_operand_aliasing={{}: (3, {})} | custom-call | tf_op jit(solution)/shard_map/pallas_call | solution.py:422
  66.4 2.1 %collective-permute-start.26 = (bf16[8,4096]{1,0:T(8,128)(2,1)S(1)}, bf16[8,4096]{1,0:T(8,128)(2,1)S(1)}, u32[]{:S(2)}, u32[]{:S(2)}) collective-permute-start(bf16[8,4096]{1,0:T(8,128)(2,1)S(1)} %fusion.9), channel_id=1, source_target_pairs={{0,24},{1,25},{2,26},{3,27},{4,28},{5,29},{6,30},{7,31},{8,16},{9,... | collective-permute-start | bytes 196616 | tf_op jit(solution)/shard_map/ppermute | solution.py:196
  68.9 2.0 %collective-permute-start.24 = (bf16[8,4096]{1,0:T(8,128)(2,1)S(1)}, bf16[8,4096]{1,0:T(8,128)(2,1)S(1)}, u32[]{:S(2)}, u32[]{:S(2)}) collective-permute-start(bf16[8,4096]{1,0:T(8,128)(2,1)S(1)} %fusion.9), channel_id=1, source_target_pairs={{0,8},{1,9},{2,10},{3,11},{4,12},{5,13},{6,14},{7,15},{8,0},{9,1},... | collective-permute-start | bytes 196616 | tf_op jit(solution)/shard_map/ppermute | solution.py:196
  70.9 1.8 %collective-permute-start.29 = (bf16[8,4096]{1,0:T(8,128)(2,1)S(1)}, bf16[8,4096]{1,0:T(8,128)(2,1)S(1)}, u32[]{:S(2)}, u32[]{:S(2)}) collective-permute-start(bf16[8,4096]{1,0:T(8,128)(2,1)S(1)} %fusion.9), channel_id=1, source_target_pairs={{0,6},{1,7},{2,4},{3,5},{4,2},{5,3},{6,0},{7,1},{8,14},{9,15},{10,... | collective-permute-start | bytes 196616 | tf_op jit(solution)/shard_map/ppermute | solution.py:196
  74.0 2.5 %collective-permute-start.27 = (bf16[32,4096]{1,0:T(8,128)(2,1)S(1)}, bf16[32,4096]{1,0:T(8,128)(2,1)S(1)}, u32[]{:S(2)}, u32[]{:S(2)}) collective-permute-start(bf16[32,4096]{1,0:T(8,128)(2,1)S(1)} %pad_maximum_fusion.refs_0_), channel_id=1, source_target_pairs={{0,2},{1,3},{2,0},{3,1},{4,6},{5,7},{6,4},{7,5},{8,10},{9,11},{10,... | collective-permute-start | bytes 786440 | tf_op jit(solution)/shard_map/ppermute | solution.py:196
  79.2 1.9 %collective-permute-done.30 = bf16[8,4096]{1,0:T(8,128)(2,1)S(1)} collective-permute-done((bf16[8,4096]{1,0:T(8,128)(2,1)S(1)}, bf16[8,4096]{1,0:T(8,128)(2,1)S(1)}, u32[]{:S(2)}, u32[]{:S(2)}) %collective-permute-start.30) | collective-permute-done | bytes 65568 | tf_op jit(solution)/shard_map/ppermute | solution.py:196
  81.0 2.0 %collective-permute-start.32 = (bf16[8,4096]{1,0:T(8,128)(2,1)S(1)}, bf16[8,4096]{1,0:T(8,128)(2,1)S(1)}, u32[]{:S(2)}, u32[]{:S(2)}) collective-permute-start(bf16[8,4096]{1,0:T(8,128)(2,1)S(1)} %collective-permute-done.29), channel_id=1, source_target_pairs={{0,24},{1,25},{2,26},{3,27},{4,28},{5,29},{6,30},{7,31},{8,16},{9,... | collective-permute-start | bytes 196616 | tf_op jit(solution)/shard_map/ppermute | solution.py:196
  84.7 2.5 %collective-permute-done.32 = bf16[8,4096]{1,0:T(8,128)(2,1)S(1)} collective-permute-done((bf16[8,4096]{1,0:T(8,128)(2,1)S(1)}, bf16[8,4096]{1,0:T(8,128)(2,1)S(1)}, u32[]{:S(2)}, u32[]{:S(2)}) %collective-permute-start.32) | collective-permute-done | bytes 65568 | tf_op jit(solution)/shard_map/ppermute | solution.py:196
  87.7 2.8 %shard_map.144.refs_13_.rows_ref = f32[256,4096]{1,0:T(8,128)S(1)} custom-call(s32[2]{0:T(128)S(1)} %pad_add_fusion.place_ref, f32[2,1,256,4096]{3,2,1,0:T(8,128)} %refs_0_.3), custom_call_target="tpu_custom_call" | custom-call | tf_op jit(solution)/shard_map/pallas_call | solution.py:255
  90.6 4.9 %shard_map.145 = (bf16[256,64]{1,0:T(8,128)(2,1)S(1)}, f32[256,512]{1,0:T(8,128)S(1)}) custom-call(s32[2]{0:T(128)S(1)} %pad_add_fusion.place_ref, bf16[32,4096]{1,0:T(8,128)(2,1)S(1)} %pad_maximum_fusion.refs_0_, bf16[32,4096]{1,0:T(8,128)(2,1)S(1)} %collective-permute-done.27.refs_1_, bf16[32,4096]{1,0:T(8,128)(2,1)S(1)} %collective-permute-done.28.refs_2_, ...), custom_call_target="tpu_custom_call" | custom-call | tf_op jit(solution)/shard_map/pallas_call | solution.py:357
  97.9 2.1 %collective-permute-start.45 = (bf16[8,4096]{1,0:T(8,128)(2,1)S(1)}, bf16[8,4096]{1,0:T(8,128)(2,1)S(1)}, u32[]{:S(2)}, u32[]{:S(2)}) collective-permute-start(bf16[8,4096]{1,0:T(8,128)(2,1)S(1)} %get-tuple-element.73), channel_id=1, source_target_pairs={{0,24},{1,25},{2,26},{3,27},{4,28},{5,29},{6,30},{7,31},{8,16},{9,... | collective-permute-start | bytes 196616 | tf_op jit(solution)/shard_map/ppermute | solution.py:196
  99.9 2.4 %collective-permute-start.43 = (bf16[8,4096]{1,0:T(8,128)(2,1)S(1)}, bf16[8,4096]{1,0:T(8,128)(2,1)S(1)}, u32[]{:S(2)}, u32[]{:S(2)}) collective-permute-start(bf16[8,4096]{1,0:T(8,128)(2,1)S(1)} %get-tuple-element.72), channel_id=1, source_target_pairs={{0,8},{1,9},{2,10},{3,11},{4,12},{5,13},{6,14},{7,15},{8,0},{9,1},... | collective-permute-start | bytes 196616 | tf_op jit(solution)/shard_map/ppermute | solution.py:196
  102.4 2.0 %collective-permute-start.38 = (bf16[32,4096]{1,0:T(8,128)(2,1)S(1)}, bf16[32,4096]{1,0:T(8,128)(2,1)S(1)}, u32[]{:S(2)}, u32[]{:S(2)}) collective-permute-start(bf16[32,4096]{1,0:T(8,128)(2,1)S(1)} %get-tuple-element.76), channel_id=1, source_target_pairs={{0,2},{1,3},{2,0},{3,1},{4,6},{5,7},{6,4},{7,5},{8,10},{9,11},{10,... | collective-permute-start | bytes 786440 | tf_op jit(solution)/shard_map/ppermute | solution.py:196
  104.6 2.7 %shard_map.146.refs_0_ = f32[2,1,256,4096]{3,2,1,0:T(8,128)} custom-call(s32[2]{0:T(128)S(1)} %pad_add_fusion.place_ref, f32[256,512]{1,0:T(8,128)S(1)} %get-tuple-element.58.vec_ref, f32[256,4096]{1,0:T(8,128)S(1)} %shard_map.144.refs_13_.rows_ref, f32[2,1,256,4096]{3,2,1,0:T(8,128)} %shard_map.143.refs_0_), custom_call_target="tpu_custom_call", output_to_operand_aliasing={{}: (3, {})} | custom-call | tf_op jit(solution)/shard_map/pallas_call | solution.py:422
  110.4 2.9 %collective-permute-done.39 = bf16[32,4096]{1,0:T(8,128)(2,1)S(1)} collective-permute-done((bf16[32,4096]{1,0:T(8,128)(2,1)S(1)}, bf16[32,4096]{1,0:T(8,128)(2,1)S(1)}, u32[]{:S(2)}, u32[]{:S(2)}) %collective-permute-start.39) | collective-permute-done | bytes 262176 | tf_op jit(solution)/shard_map/ppermute | solution.py:196
  113.7 2.3 %collective-permute-start.41 = (bf16[8,4096]{1,0:T(8,128)(2,1)S(1)}, bf16[8,4096]{1,0:T(8,128)(2,1)S(1)}, u32[]{:S(2)}, u32[]{:S(2)}) collective-permute-start(bf16[8,4096]{1,0:T(8,128)(2,1)S(1)} %get-tuple-element.83), channel_id=1, source_target_pairs={{0,16},{1,17},{2,18},{3,19},{4,20},{5,21},{6,22},{7,23},{8,24},{9,... | collective-permute-start | bytes 196616 | tf_op jit(solution)/shard_map/ppermute | solution.py:196
  116.0 1.8 %collective-permute-start.42 = (bf16[8,4096]{1,0:T(8,128)(2,1)S(1)}, bf16[8,4096]{1,0:T(8,128)(2,1)S(1)}, u32[]{:S(2)}, u32[]{:S(2)}) collective-permute-start(bf16[8,4096]{1,0:T(8,128)(2,1)S(1)} %get-tuple-element.82), channel_id=1, source_target_pairs={{0,24},{1,25},{2,26},{3,27},{4,28},{5,29},{6,30},{7,31},{8,16},{9,... | collective-permute-start | bytes 196616 | tf_op jit(solution)/shard_map/ppermute | solution.py:196
  117.8 2.6 %shard_map.147 = f32[2,1,256,4096]{3,2,1,0:T(8,128)} custom-call(s32[2]{0:T(128)S(1)} %pad_add_fusion.place_ref, f32[256,512]{1,0:T(8,128)S(1)} %get-tuple-element.58.vec_ref, f32[256,4096]{1,0:T(8,128)S(1)} %shard_map.144.refs_13_.rows_ref, f32[2,1,256,4096]{3,2,1,0:T(8,128)} %shard_map.146.refs_0_), custom_call_target="tpu_custom_call", output_to_operand_aliasing={{}: (3, {})} | custom-call | tf_op jit(solution)/shard_map/pallas_call | solution.py:422
  (108 shorter events, 34.0 us)
Async XLA Ops:
  0.7 9.2 %collective-permute-start = (bf16[8,4096]{1,0:T(8,128)(2,1)}, bf16[8,4096]{1,0:T(8,128)(2,1)S(1)}, u32[]{:S(2)}, u32[]{:S(2)}) collective-permute-start(bf16[8,4096]{1,0:T(8,128)(2,1)} %bitcast.33), channel_id=1, source_target_pairs={{0,8},{1,9},{2,10},{3,11},{4,12},{5,13},{6,14},{7,15},{8,0},{9,1},... | collective-permute-start | bytes 196616 | tf_op jit(solution)/shard_map/ppermute | solution.py:196
  3.8 7.5 %collective-permute-start.1 = (bf16[8,4096]{1,0:T(8,128)(2,1)}, bf16[8,4096]{1,0:T(8,128)(2,1)S(1)}, u32[]{:S(2)}, u32[]{:S(2)}) collective-permute-start(bf16[8,4096]{1,0:T(8,128)(2,1)} %bitcast.34), channel_id=1, source_target_pairs={{0,16},{1,17},{2,18},{3,19},{4,20},{5,21},{6,22},{7,23},{8,24},{9,... | collective-permute-start | bytes 196616 | tf_op jit(solution)/shard_map/ppermute | solution.py:196
  6.4 6.3 %collective-permute-start.2 = (bf16[8,4096]{1,0:T(8,128)(2,1)}, bf16[8,4096]{1,0:T(8,128)(2,1)S(1)}, u32[]{:S(2)}, u32[]{:S(2)}) collective-permute-start(bf16[8,4096]{1,0:T(8,128)(2,1)} %bitcast.35), channel_id=1, source_target_pairs={{0,24},{1,25},{2,26},{3,27},{4,28},{5,29},{6,30},{7,31},{8,16},{9,... | collective-permute-start | bytes 196616 | tf_op jit(solution)/shard_map/ppermute | solution.py:196
  6.4 9.3 %collective-permute-start.5 = (bf16[8,4096]{1,0:T(8,128)(2,1)}, bf16[8,4096]{1,0:T(8,128)(2,1)S(1)}, u32[]{:S(2)}, u32[]{:S(2)}) collective-permute-start(bf16[8,4096]{1,0:T(8,128)(2,1)} %bitcast.36), channel_id=1, source_target_pairs={{0,6},{1,7},{2,4},{3,5},{4,2},{5,3},{6,0},{7,1},{8,14},{9,15},{10,... | collective-permute-start | bytes 196616 | tf_op jit(solution)/shard_map/ppermute | solution.py:196
  9.0 34.7 %collective-permute-start.14 = (bf16[2,64,4096]{2,1,0:T(8,128)(2,1)}, bf16[2,64,4096]{2,1,0:T(8,128)(2,1)S(1)}, u32[]{:S(2)}, u32[]{:S(2)}) collective-permute-start(bf16[2,64,4096]{2,1,0:T(8,128)(2,1)} %bitcast.32), channel_id=1, source_target_pairs={{0,1},{1,0},{2,3},{3,2},{4,5},{5,4},{6,7},{7,6},{8,9},{9,8},{10,11... | collective-permute-start | bytes 3145736 | tf_op jit(solution)/shard_map/ppermute | solution.py:196
  12.7 19.6 %collective-permute-start.3 = (bf16[32,4096]{1,0:T(8,128)(2,1)S(1)}, bf16[32,4096]{1,0:T(8,128)(2,1)S(1)}, u32[]{:S(2)}, u32[]{:S(2)}) collective-permute-start(bf16[32,4096]{1,0:T(8,128)(2,1)S(1)} %constant_dynamic-update-slice_fusion.refs_0_), channel_id=1, source_target_pairs={{0,2},{1,3},{2,0},{3,1},{4,6},{5,7},{6,4},{7,5},{8,10},{9,11},{10,... | collective-permute-start | bytes 786440 | tf_op jit(solution)/shard_map/ppermute | solution.py:196
  14.2 18.6 %collective-permute-start.4 = (bf16[32,4096]{1,0:T(8,128)(2,1)S(1)}, bf16[32,4096]{1,0:T(8,128)(2,1)S(1)}, u32[]{:S(2)}, u32[]{:S(2)}) collective-permute-start(bf16[32,4096]{1,0:T(8,128)(2,1)S(1)} %constant_dynamic-update-slice_fusion.refs_0_), channel_id=1, source_target_pairs={{0,4},{1,5},{2,6},{3,7},{4,0},{5,1},{6,2},{7,3},{8,12},{9,13},{10,... | collective-permute-start | bytes 786440 | tf_op jit(solution)/shard_map/ppermute | solution.py:196
  15.7 21.9 %collective-permute-start.9 = (bf16[32,4096]{1,0:T(8,128)(2,1)S(1)}, bf16[32,4096]{1,0:T(8,128)(2,1)S(1)}, u32[]{:S(2)}, u32[]{:S(2)}) collective-permute-start(bf16[32,4096]{1,0:T(8,128)(2,1)S(1)} %constant_dynamic-update-slice_fusion.refs_0_), channel_id=1, source_target_pairs={{0,1},{1,0},{2,3},{3,2},{4,5},{5,4},{6,7},{7,6},{8,9},{9,8},{10,11... | collective-permute-start | bytes 786440 | tf_op jit(solution)/shard_map/ppermute | solution.py:196
  26.2 6.1 %collective-permute-start.8 = (bf16[8,4096]{1,0:T(8,128)(2,1)S(1)}, bf16[8,4096]{1,0:T(8,128)(2,1)S(1)}, u32[]{:S(2)}, u32[]{:S(2)}) collective-permute-start(bf16[8,4096]{1,0:T(8,128)(2,1)S(1)} %collective-permute-done.5), channel_id=1, source_target_pairs={{0,24},{1,25},{2,26},{3,27},{4,28},{5,29},{6,30},{7,31},{8,16},{9,... | collective-permute-start | bytes 196616 | tf_op jit(solution)/shard_map/ppermute | solution.py:196
  44.8 8.2 %collective-permute-start.22 = (bf16[8,4096]{1,0:T(8,128)(2,1)S(1)}, bf16[8,4096]{1,0:T(8,128)(2,1)S(1)}, u32[]{:S(2)}, u32[]{:S(2)}) collective-permute-start(bf16[8,4096]{1,0:T(8,128)(2,1)S(1)} %get-tuple-element.78), channel_id=1, source_target_pairs={{0,24},{1,25},{2,26},{3,27},{4,28},{5,29},{6,30},{7,31},{8,16},{9,... | collective-permute-start | bytes 196616 | tf_op jit(solution)/shard_map/ppermute | solution.py:196
  46.7 7.1 %collective-permute-start.21 = (bf16[8,4096]{1,0:T(8,128)(2,1)S(1)}, bf16[8,4096]{1,0:T(8,128)(2,1)S(1)}, u32[]{:S(2)}, u32[]{:S(2)}) collective-permute-start(bf16[8,4096]{1,0:T(8,128)(2,1)S(1)} %get-tuple-element.79), channel_id=1, source_target_pairs={{0,16},{1,17},{2,18},{3,19},{4,20},{5,21},{6,22},{7,23},{8,24},{9,... | collective-permute-start | bytes 196616 | tf_op jit(solution)/shard_map/ppermute | solution.py:196
  46.7 7.1 %collective-permute-start.20 = (bf16[8,4096]{1,0:T(8,128)(2,1)S(1)}, bf16[8,4096]{1,0:T(8,128)(2,1)S(1)}, u32[]{:S(2)}, u32[]{:S(2)}) collective-permute-start(bf16[8,4096]{1,0:T(8,128)(2,1)S(1)} %get-tuple-element.77), channel_id=1, source_target_pairs={{0,8},{1,9},{2,10},{3,11},{4,12},{5,13},{6,14},{7,15},{8,0},{9,1},... | collective-permute-start | bytes 196616 | tf_op jit(solution)/shard_map/ppermute | solution.py:196
  49.3 8.4 %collective-permute-start.15 = (bf16[32,4096]{1,0:T(8,128)(2,1)S(1)}, bf16[32,4096]{1,0:T(8,128)(2,1)S(1)}, u32[]{:S(2)}, u32[]{:S(2)}) collective-permute-start(bf16[32,4096]{1,0:T(8,128)(2,1)S(1)} %get-tuple-element.81), channel_id=1, source_target_pairs={{0,2},{1,3},{2,0},{3,1},{4,6},{5,7},{6,4},{7,5},{8,10},{9,11},{10,... | collective-permute-start | bytes 786440 | tf_op jit(solution)/shard_map/ppermute | solution.py:196
  49.9 7.8 %collective-permute-start.16 = (bf16[32,4096]{1,0:T(8,128)(2,1)S(1)}, bf16[32,4096]{1,0:T(8,128)(2,1)S(1)}, u32[]{:S(2)}, u32[]{:S(2)}) collective-permute-start(bf16[32,4096]{1,0:T(8,128)(2,1)S(1)} %get-tuple-element.80), channel_id=1, source_target_pairs={{0,4},{1,5},{2,6},{3,7},{4,0},{5,1},{6,2},{7,3},{8,12},{9,13},{10,... | collective-permute-start | bytes 786440 | tf_op jit(solution)/shard_map/ppermute | solution.py:196
  53.8 11.0 %collective-permute-start.23 = (bf16[8,4096]{1,0:T(8,128)(2,1)S(1)}, bf16[8,4096]{1,0:T(8,128)(2,1)S(1)}, u32[]{:S(2)}, u32[]{:S(2)}) collective-permute-start(bf16[8,4096]{1,0:T(8,128)(2,1)S(1)} %add_convert_fusion.1), channel_id=1, source_target_pairs={{0,6},{1,7},{2,4},{3,5},{4,2},{5,3},{6,0},{7,1},{8,14},{9,15},{10,... | collective-permute-start | bytes 196616 | tf_op jit(solution)/shard_map/ppermute | solution.py:196
  57.8 7.1 %collective-permute-start.17 = (bf16[8,4096]{1,0:T(8,128)(2,1)S(1)}, bf16[8,4096]{1,0:T(8,128)(2,1)S(1)}, u32[]{:S(2)}, u32[]{:S(2)}) collective-permute-start(bf16[8,4096]{1,0:T(8,128)(2,1)S(1)} %get-tuple-element.87), channel_id=1, source_target_pairs={{0,8},{1,9},{2,10},{3,11},{4,12},{5,13},{6,14},{7,15},{8,0},{9,1},... | collective-permute-start | bytes 196616 | tf_op jit(solution)/shard_map/ppermute | solution.py:196
  58.5 6.4 %collective-permute-start.18 = (bf16[8,4096]{1,0:T(8,128)(2,1)S(1)}, bf16[8,4096]{1,0:T(8,128)(2,1)S(1)}, u32[]{:S(2)}, u32[]{:S(2)}) collective-permute-start(bf16[8,4096]{1,0:T(8,128)(2,1)S(1)} %get-tuple-element.86), channel_id=1, source_target_pairs={{0,16},{1,17},{2,18},{3,19},{4,20},{5,21},{6,22},{7,23},{8,24},{9,... | collective-permute-start | bytes 196616 | tf_op jit(solution)/shard_map/ppermute | solution.py:196
  60.2 6.2 %collective-permute-start.19 = (bf16[8,4096]{1,0:T(8,128)(2,1)S(1)}, bf16[8,4096]{1,0:T(8,128)(2,1)S(1)}, u32[]{:S(2)}, u32[]{:S(2)}) collective-permute-start(bf16[8,4096]{1,0:T(8,128)(2,1)S(1)} %get-tuple-element.85), channel_id=1, source_target_pairs={{0,24},{1,25},{2,26},{3,27},{4,28},{5,29},{6,30},{7,31},{8,16},{9,... | collective-permute-start | bytes 196616 | tf_op jit(solution)/shard_map/ppermute | solution.py:196
  66.4 6.2 %collective-permute-start.26 = (bf16[8,4096]{1,0:T(8,128)(2,1)S(1)}, bf16[8,4096]{1,0:T(8,128)(2,1)S(1)}, u32[]{:S(2)}, u32[]{:S(2)}) collective-permute-start(bf16[8,4096]{1,0:T(8,128)(2,1)S(1)} %fusion.9), channel_id=1, source_target_pairs={{0,24},{1,25},{2,26},{3,27},{4,28},{5,29},{6,30},{7,31},{8,16},{9,... | collective-permute-start | bytes 196616 | tf_op jit(solution)/shard_map/ppermute | solution.py:196
  74.0 13.1 %collective-permute-start.27 = (bf16[32,4096]{1,0:T(8,128)(2,1)S(1)}, bf16[32,4096]{1,0:T(8,128)(2,1)S(1)}, u32[]{:S(2)}, u32[]{:S(2)}) collective-permute-start(bf16[32,4096]{1,0:T(8,128)(2,1)S(1)} %pad_maximum_fusion.refs_0_), channel_id=1, source_target_pairs={{0,2},{1,3},{2,0},{3,1},{4,6},{5,7},{6,4},{7,5},{8,10},{9,11},{10,... | collective-permute-start | bytes 786440 | tf_op jit(solution)/shard_map/ppermute | solution.py:196
  76.5 11.1 %collective-permute-start.28 = (bf16[32,4096]{1,0:T(8,128)(2,1)S(1)}, bf16[32,4096]{1,0:T(8,128)(2,1)S(1)}, u32[]{:S(2)}, u32[]{:S(2)}) collective-permute-start(bf16[32,4096]{1,0:T(8,128)(2,1)S(1)} %pad_maximum_fusion.refs_0_), channel_id=1, source_target_pairs={{0,4},{1,5},{2,6},{3,7},{4,0},{5,1},{6,2},{7,3},{8,12},{9,13},{10,... | collective-permute-start | bytes 786440 | tf_op jit(solution)/shard_map/ppermute | solution.py:196
  76.5 14.0 %collective-permute-start.33 = (bf16[32,4096]{1,0:T(8,128)(2,1)S(1)}, bf16[32,4096]{1,0:T(8,128)(2,1)S(1)}, u32[]{:S(2)}, u32[]{:S(2)}) collective-permute-start(bf16[32,4096]{1,0:T(8,128)(2,1)S(1)} %pad_maximum_fusion.refs_0_), channel_id=1, source_target_pairs={{0,1},{1,0},{2,3},{3,2},{4,5},{5,4},{6,7},{7,6},{8,9},{9,8},{10,11... | collective-permute-start | bytes 786440 | tf_op jit(solution)/shard_map/ppermute | solution.py:196
  77.8 6.9 %collective-permute-start.31 = (bf16[8,4096]{1,0:T(8,128)(2,1)S(1)}, bf16[8,4096]{1,0:T(8,128)(2,1)S(1)}, u32[]{:S(2)}, u32[]{:S(2)}) collective-permute-start(bf16[8,4096]{1,0:T(8,128)(2,1)S(1)} %collective-permute-done.29), channel_id=1, source_target_pairs={{0,16},{1,17},{2,18},{3,19},{4,20},{5,21},{6,22},{7,23},{8,24},{9,... | collective-permute-start | bytes 196616 | tf_op jit(solution)/shard_map/ppermute | solution.py:196
  81.0 6.1 %collective-permute-start.32 = (bf16[8,4096]{1,0:T(8,128)(2,1)S(1)}, bf16[8,4096]{1,0:T(8,128)(2,1)S(1)}, u32[]{:S(2)}, u32[]{:S(2)}) collective-permute-start(bf16[8,4096]{1,0:T(8,128)(2,1)S(1)} %collective-permute-done.29), channel_id=1, source_target_pairs={{0,24},{1,25},{2,26},{3,27},{4,28},{5,29},{6,30},{7,31},{8,16},{9,... | collective-permute-start | bytes 196616 | tf_op jit(solution)/shard_map/ppermute | solution.py:196
  97.9 9.4 %collective-permute-start.45 = (bf16[8,4096]{1,0:T(8,128)(2,1)S(1)}, bf16[8,4096]{1,0:T(8,128)(2,1)S(1)}, u32[]{:S(2)}, u32[]{:S(2)}) collective-permute-start(bf16[8,4096]{1,0:T(8,128)(2,1)S(1)} %get-tuple-element.73), channel_id=1, source_target_pairs={{0,24},{1,25},{2,26},{3,27},{4,28},{5,29},{6,30},{7,31},{8,16},{9,... | collective-permute-start | bytes 196616 | tf_op jit(solution)/shard_map/ppermute | solution.py:196
  99.9 7.3 %collective-permute-start.44 = (bf16[8,4096]{1,0:T(8,128)(2,1)S(1)}, bf16[8,4096]{1,0:T(8,128)(2,1)S(1)}, u32[]{:S(2)}, u32[]{:S(2)}) collective-permute-start(bf16[8,4096]{1,0:T(8,128)(2,1)S(1)} %get-tuple-element.74), channel_id=1, source_target_pairs={{0,16},{1,17},{2,18},{3,19},{4,20},{5,21},{6,22},{7,23},{8,24},{9,... | collective-permute-start | bytes 196616 | tf_op jit(solution)/shard_map/ppermute | solution.py:196
  99.9 7.4 %collective-permute-start.43 = (bf16[8,4096]{1,0:T(8,128)(2,1)S(1)}, bf16[8,4096]{1,0:T(8,128)(2,1)S(1)}, u32[]{:S(2)}, u32[]{:S(2)}) collective-permute-start(bf16[8,4096]{1,0:T(8,128)(2,1)S(1)} %get-tuple-element.72), channel_id=1, source_target_pairs={{0,8},{1,9},{2,10},{3,11},{4,12},{5,13},{6,14},{7,15},{8,0},{9,1},... | collective-permute-start | bytes 196616 | tf_op jit(solution)/shard_map/ppermute | solution.py:196
  102.4 8.0 %collective-permute-start.38 = (bf16[32,4096]{1,0:T(8,128)(2,1)S(1)}, bf16[32,4096]{1,0:T(8,128)(2,1)S(1)}, u32[]{:S(2)}, u32[]{:S(2)}) collective-permute-start(bf16[32,4096]{1,0:T(8,128)(2,1)S(1)} %get-tuple-element.76), channel_id=1, source_target_pairs={{0,2},{1,3},{2,0},{3,1},{4,6},{5,7},{6,4},{7,5},{8,10},{9,11},{10,... | collective-permute-start | bytes 786440 | tf_op jit(solution)/shard_map/ppermute | solution.py:196
  104.4 8.8 %collective-permute-start.39 = (bf16[32,4096]{1,0:T(8,128)(2,1)S(1)}, bf16[32,4096]{1,0:T(8,128)(2,1)S(1)}, u32[]{:S(2)}, u32[]{:S(2)}) collective-permute-start(bf16[32,4096]{1,0:T(8,128)(2,1)S(1)} %get-tuple-element.75), channel_id=1, source_target_pairs={{0,4},{1,5},{2,6},{3,7},{4,0},{5,1},{6,2},{7,3},{8,12},{9,13},{10,... | collective-permute-start | bytes 786440 | tf_op jit(solution)/shard_map/ppermute | solution.py:196
  107.3 13.1 %collective-permute-start.46 = (bf16[8,4096]{1,0:T(8,128)(2,1)S(1)}, bf16[8,4096]{1,0:T(8,128)(2,1)S(1)}, u32[]{:S(2)}, u32[]{:S(2)}) collective-permute-start(bf16[8,4096]{1,0:T(8,128)(2,1)S(1)} %add_convert_fusion), channel_id=1, source_target_pairs={{0,6},{1,7},{2,4},{3,5},{4,2},{5,3},{6,0},{7,1},{8,14},{9,15},{10,... | collective-permute-start | bytes 196616 | tf_op jit(solution)/shard_map/ppermute | solution.py:196
  113.4 7.1 %collective-permute-start.40 = (bf16[8,4096]{1,0:T(8,128)(2,1)S(1)}, bf16[8,4096]{1,0:T(8,128)(2,1)S(1)}, u32[]{:S(2)}, u32[]{:S(2)}) collective-permute-start(bf16[8,4096]{1,0:T(8,128)(2,1)S(1)} %get-tuple-element.84), channel_id=1, source_target_pairs={{0,8},{1,9},{2,10},{3,11},{4,12},{5,13},{6,14},{7,15},{8,0},{9,1},... | collective-permute-start | bytes 196616 | tf_op jit(solution)/shard_map/ppermute | solution.py:196
  113.7 6.8 %collective-permute-start.41 = (bf16[8,4096]{1,0:T(8,128)(2,1)S(1)}, bf16[8,4096]{1,0:T(8,128)(2,1)S(1)}, u32[]{:S(2)}, u32[]{:S(2)}) collective-permute-start(bf16[8,4096]{1,0:T(8,128)(2,1)S(1)} %get-tuple-element.83), channel_id=1, source_target_pairs={{0,16},{1,17},{2,18},{3,19},{4,20},{5,21},{6,22},{7,23},{8,24},{9,... | collective-permute-start | bytes 196616 | tf_op jit(solution)/shard_map/ppermute | solution.py:196
  (17 other events, 73.4 us)

commit v2 on v1

--- a/solution.py
+++ b/solution.py
@@ -190,6 +190,7 @@
 CORES = 2
 PLANE = 4
 STATE_ROWS = 64
+FRONT_ROWS = 256
 
 
 def moved(part, mask):
@@ -323,16 +324,16 @@
     kn_wide, decay_r_wide = twice(kn), twice(decay_r)
     repeats = columns // wide
     removed, kept = [], []
-    for block in range(seqs // STATE_ROWS):
-        span = slice(block * STATE_ROWS, (block + 1) * STATE_ROWS)
+    for block in range(seqs // FRONT_ROWS):
+        span = slice(block * FRONT_ROWS, (block + 1) * FRONT_ROWS)
         rows = rows_ref[span, :]
         by_kn = (rows * jnp.tile(kn_wide[span], (1, repeats))).astype(jnp.bfloat16)
         by_r = (rows * jnp.tile(decay_r_wide[span], (1, repeats))).astype(jnp.bfloat16)
         both = jnp.dot(
             jnp.concatenate([by_kn, by_r], 0), fold_ref[...], preferred_element_type=jnp.float32
         )
-        removed.append(both[:STATE_ROWS, :head_size])
-        kept.append(both[STATE_ROWS:, :head_size])
+        removed.append(both[:FRONT_ROWS, :head_size])
+        kept.append(both[FRONT_ROWS:, :head_size])
     removed, kept = jnp.concatenate(removed, 0), jnp.concatenate(kept, 0)
     kn_rate = kn * rate
     k_rate = k * rate
@@ -460,16 +461,15 @@
     block = levels * rows
     step = CORES * PLANE
     wide = lambda got: [part.astype(jnp.float32) for part in got]
-    sends = parts.astype(jnp.bfloat16)
-    across = [moved(sends[q * block : (q + 1) * block], CORES * q) for q in (1, 2)]
-    diagonal = sends[3 * block :]
+    across = [moved(parts[q * block : (q + 1) * block], CORES * q) for q in (1, 2)]
+    diagonal = parts[3 * block :]
     along = [moved(diagonal[at * rows : (at + 1) * rows], step * at) for at in range(1, levels)]
     new_state = update_part(new_state, 0)
     *across, new_state = lax.optimization_barrier((*across, new_state))
-    summed = parts[:block] + sum(wide(across))
+    summed = sum(wide([parts[:block], *across]))
     sends = summed.astype(jnp.bfloat16)
     got = [moved(sends[at * rows : (at + 1) * rows], step * at) for at in range(1, levels)]
-    corner = (parts[3 * block : 3 * block + rows] + sum(wide(along))).astype(jnp.bfloat16)
+    corner = sum(wide([diagonal[:rows], *along])).astype(jnp.bfloat16)
     got.append(moved(corner, CORES * 3))
     new_state = update_part(new_state, 1)
     *got, new_state = lax.optimization_barrier((*got, new_state))
@@ -524,7 +524,10 @@
         out, vec = front(place, pieces, places, gain, tables, packed[layer], rows, layer)
         half = out.shape[0] // CORES
         parts = jnp.dot(out[:half], own_out[layer], preferred_element_type=jnp.float32)
-        parts += jnp.dot(moved(out[half:], 1), other_out[layer], preferred_element_type=jnp.float32)
+        swapped = moved(out[half:], 1)
+        parts = lax.optimization_barrier(parts)
+        parts += jnp.dot(swapped, other_out[layer], preferred_element_type=jnp.float32)
+        parts = parts.astype(jnp.bfloat16)
         parts, vec = lax.optimization_barrier((parts, vec))
         update_part = lambda previous, part: update(
             place, vec, rows, previous, state.shape, layer, part

time: 123 us -> 121 us (0.984)
  Pallas kernels: 27.8 us -> 26.1 us
    pallas_call x2, Pallas kernels: 9.66 us -> 7.99 us  [front(): pl.pallas_call(partial(front_kernel, piece_rows=piece_rows, head_size=hea...]
  transfers between devices with their start and end apart: 47 -> 47, of which waited for: 17 -> 17; matrix products, arithmetic and copies ran while one was open for 1% -> 2% of each run, Pallas kernels for 19% -> 18%
where the time goes in v2:
time: 121 us; the launch traced here: 120 us
  starting transfers between devices  54.6 us (45%)
  waiting for transfers between devices  34.3 us (28%)
  Pallas kernels  26.1 us (22%)
  matrix products  1.64 us (1%)
  other arithmetic  1.52 us (1%)
    ppermute x47, starting transfers between devices, moved(): lax.ppermute(part, 'tp', [(i, i ^ mask) for i in range(lax.axis_size('tp'...  54.6 us
    ppermute x47, waiting for transfers between devices, moved(): lax.ppermute(part, 'tp', [(i, i ^ mask) for i in range(lax.axis_size('tp'...  34.3 us
    pallas_call x4, Pallas kernels, update(): pl.pallas_call(partial(update_kernel, seq_tile=seqs // lax.axis_size('tp'...  10.6 us
    pallas_call x2, Pallas kernels, front(): pl.pallas_call(partial(front_kernel, piece_rows=piece_rows, head_size=hea...  7.99 us
    pallas_call x2, Pallas kernels, load(): pl.pallas_call(partial(load_kernel, layer=layer, layers=layers, count=len...  7.57 us
  transfers between devices with their start and end apart: 47, of which 17 were waited for; matrix products, arithmetic and copies ran while one was open for 2% of the time, Pallas kernels for 18%

profile of v2, /device:TPU:0, one launch (start us, length us, event | category | flops | bytes accessed | tf_op | source)
XLA Modules:
  0.0 120.3 jit_solution(13336648226949324229)
XLA Ops:
  0.7 3.1 %collective-permute-start = (bf16[8,4096]{1,0:T(8,128)(2,1)}, bf16[8,4096]{1,0:T(8,128)(2,1)S(1)}, u32[]{:S(2)}, u32[]{:S(2)}) collective-permute-start(bf16[8,4096]{1,0:T(8,128)(2,1)} %bitcast.33), channel_id=1, source_target_pairs={{0,8},{1,9},{2,10},{3,11},{4,12},{5,13},{6,14},{7,15},{8,0},{9,1},... | collective-permute-start | bytes 196616 | tf_op jit(solution)/shard_map/ppermute | solution.py:197
  3.8 2.6 %collective-permute-start.1 = (bf16[8,4096]{1,0:T(8,128)(2,1)}, bf16[8,4096]{1,0:T(8,128)(2,1)S(1)}, u32[]{:S(2)}, u32[]{:S(2)}) collective-permute-start(bf16[8,4096]{1,0:T(8,128)(2,1)} %bitcast.34), channel_id=1, source_target_pairs={{0,16},{1,17},{2,18},{3,19},{4,20},{5,21},{6,22},{7,23},{8,24},{9,... | collective-permute-start | bytes 196616 | tf_op jit(solution)/shard_map/ppermute | solution.py:197
  6.4 2.7 %collective-permute-start.5 = (bf16[8,4096]{1,0:T(8,128)(2,1)}, bf16[8,4096]{1,0:T(8,128)(2,1)S(1)}, u32[]{:S(2)}, u32[]{:S(2)}) collective-permute-start(bf16[8,4096]{1,0:T(8,128)(2,1)} %bitcast.36), channel_id=1, source_target_pairs={{0,6},{1,7},{2,4},{3,5},{4,2},{5,3},{6,0},{7,1},{8,14},{9,15},{10,... | collective-permute-start | bytes 196616 | tf_op jit(solution)/shard_map/ppermute | solution.py:197
  15.7 4.5 %collective-permute-done.6 = bf16[8,4096]{1,0:T(8,128)(2,1)S(1)} collective-permute-done((bf16[8,4096]{1,0:T(8,128)(2,1)S(1)}, bf16[8,4096]{1,0:T(8,128)(2,1)S(1)}, u32[]{:S(2)}, u32[]{:S(2)}) %collective-permute-start.6) | collective-permute-done | bytes 65568 | tf_op jit(solution)/shard_map/ppermute | solution.py:197
  21.8 4.4 %collective-permute-done.7 = bf16[8,4096]{1,0:T(8,128)(2,1)S(1)} collective-permute-done((bf16[8,4096]{1,0:T(8,128)(2,1)S(1)}, bf16[8,4096]{1,0:T(8,128)(2,1)S(1)}, u32[]{:S(2)}, u32[]{:S(2)}) %collective-permute-start.7) | collective-permute-done | bytes 65568 | tf_op jit(solution)/shard_map/ppermute | solution.py:197
  26.2 1.8 %collective-permute-start.8 = (bf16[8,4096]{1,0:T(8,128)(2,1)S(1)}, bf16[8,4096]{1,0:T(8,128)(2,1)S(1)}, u32[]{:S(2)}, u32[]{:S(2)}) collective-permute-start(bf16[8,4096]{1,0:T(8,128)(2,1)S(1)} %collective-permute-done.5), channel_id=1, source_target_pairs={{0,24},{1,25},{2,26},{3,27},{4,28},{5,29},{6,30},{7,31},{8,16},{9,... | collective-permute-start | bytes 196616 | tf_op jit(solution)/shard_map/ppermute | solution.py:197
  28.0 4.2 %collective-permute-done.8 = bf16[8,4096]{1,0:T(8,128)(2,1)S(1)} collective-permute-done((bf16[8,4096]{1,0:T(8,128)(2,1)S(1)}, bf16[8,4096]{1,0:T(8,128)(2,1)S(1)}, u32[]{:S(2)}, u32[]{:S(2)}) %collective-permute-start.8) | collective-permute-done | bytes 65568 | tf_op jit(solution)/shard_map/ppermute | solution.py:197
  32.8 4.8 %shard_map.140 = (f32[256,4096]{1,0:T(8,128)S(1)}, bf16[384,4096]{1,0:T(8,128)(2,1)S(1)}, bf16[384,4096]{1,0:T(8,128)(2,1)S(1)}, f32[2,4096]{1,0:T(2,128)S(1)}, ...) custom-call(s32[2]{0:T(128)S(1)} %pad_add_fusion.place_ref, f32[2,1,256,4096]{3,2,1,0:T(8,128)} %refs_0_.3, ...), custom_call_target="tpu_custom_call" | custom-call | tf_op jit(solution)/shard_map/pallas_call | solution.py:256
  37.7 3.9 %shard_map.141 = (bf16[256,64]{1,0:T(8,128)(2,1)S(1)}, f32[256,512]{1,0:T(8,128)S(1)}) custom-call(s32[2]{0:T(128)S(1)} %pad_add_fusion.place_ref, bf16[32,4096]{1,0:T(8,128)(2,1)S(1)} %constant_dynamic-update-slice_fusion.refs_0_, bf16[32,4096]{1,0:T(8,128)(2,1)S(1)} %collective-permute-done.3.refs_1_, bf16[32,4096]{1,0:T(8,128)(2,1)S(1)} %collective-permute-done.4.refs_2_, ...), custom_call_target="tpu_custom_call" | custom-call | tf_op jit(solution)/shard_map/pallas_call | solution.py:358
  43.6 1.9 %collective-permute-start.22 = (bf16[8,4096]{1,0:T(8,128)(2,1)S(1)}, bf16[8,4096]{1,0:T(8,128)(2,1)S(1)}, u32[]{:S(2)}, u32[]{:S(2)}) collective-permute-start(bf16[8,4096]{1,0:T(8,128)(2,1)S(1)} %get-tuple-element.78), channel_id=1, source_target_pairs={{0,24},{1,25},{2,26},{3,27},{4,28},{5,29},{6,30},{7,31},{8,16},{9,... | collective-permute-start | bytes 196616 | tf_op jit(solution)/shard_map/ppermute | solution.py:197
  45.5 2.5 %collective-permute-start.20 = (bf16[8,4096]{1,0:T(8,128)(2,1)S(1)}, bf16[8,4096]{1,0:T(8,128)(2,1)S(1)}, u32[]{:S(2)}, u32[]{:S(2)}) collective-permute-start(bf16[8,4096]{1,0:T(8,128)(2,1)S(1)} %get-tuple-element.77), channel_id=1, source_target_pairs={{0,8},{1,9},{2,10},{3,11},{4,12},{5,13},{6,14},{7,15},{8,0},{9,1},... | collective-permute-start | bytes 196616 | tf_op jit(solution)/shard_map/ppermute | solution.py:197
  49.2 2.6 %shard_map.142.refs_0_ = f32[2,1,256,4096]{3,2,1,0:T(8,128)} custom-call(s32[2]{0:T(128)S(1)} %pad_add_fusion.place_ref, f32[256,512]{1,0:T(8,128)S(1)} %get-tuple-element.46.vec_ref, f32[256,4096]{1,0:T(8,128)S(1)} %get-tuple-element.42.refs_13_.rows_ref), custom_call_target="tpu_custom_call" | custom-call | tf_op jit(solution)/shard_map/pallas_call | solution.py:423
  52.6 1.8 %collective-permute-start.23 = (bf16[8,4096]{1,0:T(8,128)(2,1)S(1)}, bf16[8,4096]{1,0:T(8,128)(2,1)S(1)}, u32[]{:S(2)}, u32[]{:S(2)}) collective-permute-start(bf16[8,4096]{1,0:T(8,128)(2,1)S(1)} %add_convert_fusion.3), channel_id=1, source_target_pairs={{0,6},{1,7},{2,4},{3,5},{4,2},{5,3},{6,0},{7,1},{8,14},{9,15},{10,... | collective-permute-start | bytes 196616 | tf_op jit(solution)/shard_map/ppermute | solution.py:197
  54.4 2.0 %collective-permute-done.15 = bf16[32,4096]{1,0:T(8,128)(2,1)S(1)} collective-permute-done((bf16[32,4096]{1,0:T(8,128)(2,1)S(1)}, bf16[32,4096]{1,0:T(8,128)(2,1)S(1)}, u32[]{:S(2)}, u32[]{:S(2)}) %collective-permute-start.15) | collective-permute-done | bytes 262176 | tf_op jit(solution)/shard_map/ppermute | solution.py:197
  59.0 2.0 %collective-permute-start.19 = (bf16[8,4096]{1,0:T(8,128)(2,1)S(1)}, bf16[8,4096]{1,0:T(8,128)(2,1)S(1)}, u32[]{:S(2)}, u32[]{:S(2)}) collective-permute-start(bf16[8,4096]{1,0:T(8,128)(2,1)S(1)} %get-tuple-element.85), channel_id=1, source_target_pairs={{0,24},{1,25},{2,26},{3,27},{4,28},{5,29},{6,30},{7,31},{8,16},{9,... | collective-permute-start | bytes 196616 | tf_op jit(solution)/shard_map/ppermute | solution.py:197
  61.0 2.6 %shard_map.143.refs_0_ = f32[2,1,256,4096]{3,2,1,0:T(8,128)} custom-call(s32[2]{0:T(128)S(1)} %pad_add_fusion.place_ref, f32[256,512]{1,0:T(8,128)S(1)} %get-tuple-element.46.vec_ref, f32[256,4096]{1,0:T(8,128)S(1)} %get-tuple-element.42.refs_13_.rows_ref, f32[2,1,256,4096]{3,2,1,0:T(8,128)} %shard_map.142.refs_0_), custom_call_target="tpu_custom_call", output_to_operand_aliasing={{}: (3, {})} | custom-call | tf_op jit(solution)/shard_map/pallas_call | solution.py:423
  65.3 2.0 %collective-permute-start.26 = (bf16[8,4096]{1,0:T(8,128)(2,1)S(1)}, bf16[8,4096]{1,0:T(8,128)(2,1)S(1)}, u32[]{:S(2)}, u32[]{:S(2)}) collective-permute-start(bf16[8,4096]{1,0:T(8,128)(2,1)S(1)} %fusion.11), channel_id=1, source_target_pairs={{0,24},{1,25},{2,26},{3,27},{4,28},{5,29},{6,30},{7,31},{8,16},{9,... | collective-permute-start | bytes 196616 | tf_op jit(solution)/shard_map/ppermute | solution.py:197
  67.7 2.0 %collective-permute-start.24 = (bf16[8,4096]{1,0:T(8,128)(2,1)S(1)}, bf16[8,4096]{1,0:T(8,128)(2,1)S(1)}, u32[]{:S(2)}, u32[]{:S(2)}) collective-permute-start(bf16[8,4096]{1,0:T(8,128)(2,1)S(1)} %fusion.11), channel_id=1, source_target_pairs={{0,8},{1,9},{2,10},{3,11},{4,12},{5,13},{6,14},{7,15},{8,0},{9,1},... | collective-permute-start | bytes 196616 | tf_op jit(solution)/shard_map/ppermute | solution.py:197
  72.8 2.5 %collective-permute-start.27 = (bf16[32,4096]{1,0:T(8,128)(2,1)S(1)}, bf16[32,4096]{1,0:T(8,128)(2,1)S(1)}, u32[]{:S(2)}, u32[]{:S(2)}) collective-permute-start(bf16[32,4096]{1,0:T(8,128)(2,1)S(1)} %pad_maximum_fusion.refs_0_), channel_id=1, source_target_pairs={{0,2},{1,3},{2,0},{3,1},{4,6},{5,7},{6,4},{7,5},{8,10},{9,11},{10,... | collective-permute-start | bytes 786440 | tf_op jit(solution)/shard_map/ppermute | solution.py:197
  78.0 1.9 %collective-permute-done.30 = bf16[8,4096]{1,0:T(8,128)(2,1)S(1)} collective-permute-done((bf16[8,4096]{1,0:T(8,128)(2,1)S(1)}, bf16[8,4096]{1,0:T(8,128)(2,1)S(1)}, u32[]{:S(2)}, u32[]{:S(2)}) %collective-permute-start.30) | collective-permute-done | bytes 65568 | tf_op jit(solution)/shard_map/ppermute | solution.py:197
  79.9 2.0 %collective-permute-start.32 = (bf16[8,4096]{1,0:T(8,128)(2,1)S(1)}, bf16[8,4096]{1,0:T(8,128)(2,1)S(1)}, u32[]{:S(2)}, u32[]{:S(2)}) collective-permute-start(bf16[8,4096]{1,0:T(8,128)(2,1)S(1)} %collective-permute-done.29), channel_id=1, source_target_pairs={{0,24},{1,25},{2,26},{3,27},{4,28},{5,29},{6,30},{7,31},{8,16},{9,... | collective-permute-start | bytes 196616 | tf_op jit(solution)/shard_map/ppermute | solution.py:197
  83.5 2.5 %collective-permute-done.32 = bf16[8,4096]{1,0:T(8,128)(2,1)S(1)} collective-permute-done((bf16[8,4096]{1,0:T(8,128)(2,1)S(1)}, bf16[8,4096]{1,0:T(8,128)(2,1)S(1)}, u32[]{:S(2)}, u32[]{:S(2)}) %collective-permute-start.32) | collective-permute-done | bytes 65568 | tf_op jit(solution)/shard_map/ppermute | solution.py:197
  86.6 2.8 %shard_map.144.refs_13_.rows_ref = f32[256,4096]{1,0:T(8,128)S(1)} custom-call(s32[2]{0:T(128)S(1)} %pad_add_fusion.place_ref, f32[2,1,256,4096]{3,2,1,0:T(8,128)} %refs_0_.3), custom_call_target="tpu_custom_call" | custom-call | tf_op jit(solution)/shard_map/pallas_call | solution.py:256
  89.4 4.1 %shard_map.145 = (bf16[256,64]{1,0:T(8,128)(2,1)S(1)}, f32[256,512]{1,0:T(8,128)S(1)}) custom-call(s32[2]{0:T(128)S(1)} %pad_add_fusion.place_ref, bf16[32,4096]{1,0:T(8,128)(2,1)S(1)} %pad_maximum_fusion.refs_0_, bf16[32,4096]{1,0:T(8,128)(2,1)S(1)} %collective-permute-done.27.refs_1_, bf16[32,4096]{1,0:T(8,128)(2,1)S(1)} %collective-permute-done.28.refs_2_, ...), custom_call_target="tpu_custom_call" | custom-call | tf_op jit(solution)/shard_map/pallas_call | solution.py:358
  95.5 2.0 %collective-permute-start.45 = (bf16[8,4096]{1,0:T(8,128)(2,1)S(1)}, bf16[8,4096]{1,0:T(8,128)(2,1)S(1)}, u32[]{:S(2)}, u32[]{:S(2)}) collective-permute-start(bf16[8,4096]{1,0:T(8,128)(2,1)S(1)} %get-tuple-element.73), channel_id=1, source_target_pairs={{0,24},{1,25},{2,26},{3,27},{4,28},{5,29},{6,30},{7,31},{8,16},{9,... | collective-permute-start | bytes 196616 | tf_op jit(solution)/shard_map/ppermute | solution.py:197
  97.5 2.4 %collective-permute-start.43 = (bf16[8,4096]{1,0:T(8,128)(2,1)S(1)}, bf16[8,4096]{1,0:T(8,128)(2,1)S(1)}, u32[]{:S(2)}, u32[]{:S(2)}) collective-permute-start(bf16[8,4096]{1,0:T(8,128)(2,1)S(1)} %get-tuple-element.72), channel_id=1, source_target_pairs={{0,8},{1,9},{2,10},{3,11},{4,12},{5,13},{6,14},{7,15},{8,0},{9,1},... | collective-permute-start | bytes 196616 | tf_op jit(solution)/shard_map/ppermute | solution.py:197
  100.0 2.0 %collective-permute-start.38 = (bf16[32,4096]{1,0:T(8,128)(2,1)S(1)}, bf16[32,4096]{1,0:T(8,128)(2,1)S(1)}, u32[]{:S(2)}, u32[]{:S(2)}) collective-permute-start(bf16[32,4096]{1,0:T(8,128)(2,1)S(1)} %get-tuple-element.76), channel_id=1, source_target_pairs={{0,2},{1,3},{2,0},{3,1},{4,6},{5,7},{6,4},{7,5},{8,10},{9,11},{10,... | collective-permute-start | bytes 786440 | tf_op jit(solution)/shard_map/ppermute | solution.py:197
  102.2 2.7 %shard_map.146.refs_0_ = f32[2,1,256,4096]{3,2,1,0:T(8,128)} custom-call(s32[2]{0:T(128)S(1)} %pad_add_fusion.place_ref, f32[256,512]{1,0:T(8,128)S(1)} %get-tuple-element.58.vec_ref, f32[256,4096]{1,0:T(8,128)S(1)} %shard_map.144.refs_13_.rows_ref, f32[2,1,256,4096]{3,2,1,0:T(8,128)} %shard_map.143.refs_0_), custom_call_target="tpu_custom_call", output_to_operand_aliasing={{}: (3, {})} | custom-call | tf_op jit(solution)/shard_map/pallas_call | solution.py:423
  108.0 2.9 %collective-permute-done.39 = bf16[32,4096]{1,0:T(8,128)(2,1)S(1)} collective-permute-done((bf16[32,4096]{1,0:T(8,128)(2,1)S(1)}, bf16[32,4096]{1,0:T(8,128)(2,1)S(1)}, u32[]{:S(2)}, u32[]{:S(2)}) %collective-permute-start.39) | collective-permute-done | bytes 262176 | tf_op jit(solution)/shard_map/ppermute | solution.py:197
  111.3 2.3 %collective-permute-start.41 = (bf16[8,4096]{1,0:T(8,128)(2,1)S(1)}, bf16[8,4096]{1,0:T(8,128)(2,1)S(1)}, u32[]{:S(2)}, u32[]{:S(2)}) collective-permute-start(bf16[8,4096]{1,0:T(8,128)(2,1)S(1)} %get-tuple-element.83), channel_id=1, source_target_pairs={{0,16},{1,17},{2,18},{3,19},{4,20},{5,21},{6,22},{7,23},{8,24},{9,... | collective-permute-start | bytes 196616 | tf_op jit(solution)/shard_map/ppermute | solution.py:197
  113.6 1.8 %collective-permute-start.42 = (bf16[8,4096]{1,0:T(8,128)(2,1)S(1)}, bf16[8,4096]{1,0:T(8,128)(2,1)S(1)}, u32[]{:S(2)}, u32[]{:S(2)}) collective-permute-start(bf16[8,4096]{1,0:T(8,128)(2,1)S(1)} %get-tuple-element.82), channel_id=1, source_target_pairs={{0,24},{1,25},{2,26},{3,27},{4,28},{5,29},{6,30},{7,31},{8,16},{9,... | collective-permute-start | bytes 196616 | tf_op jit(solution)/shard_map/ppermute | solution.py:197
  115.4 2.6 %shard_map.147 = f32[2,1,256,4096]{3,2,1,0:T(8,128)} custom-call(s32[2]{0:T(128)S(1)} %pad_add_fusion.place_ref, f32[256,512]{1,0:T(8,128)S(1)} %get-tuple-element.58.vec_ref, f32[256,4096]{1,0:T(8,128)S(1)} %shard_map.144.refs_13_.rows_ref, f32[2,1,256,4096]{3,2,1,0:T(8,128)} %shard_map.146.refs_0_), custom_call_target="tpu_custom_call", output_to_operand_aliasing={{}: (3, {})} | custom-call | tf_op jit(solution)/shard_map/pallas_call | solution.py:423
  (108 shorter events, 33.4 us)
Async XLA Ops:
  0.7 9.2 %collective-permute-start = (bf16[8,4096]{1,0:T(8,128)(2,1)}, bf16[8,4096]{1,0:T(8,128)(2,1)S(1)}, u32[]{:S(2)}, u32[]{:S(2)}) collective-permute-start(bf16[8,4096]{1,0:T(8,128)(2,1)} %bitcast.33), channel_id=1, source_target_pairs={{0,8},{1,9},{2,10},{3,11},{4,12},{5,13},{6,14},{7,15},{8,0},{9,1},... | collective-permute-start | bytes 196616 | tf_op jit(solution)/shard_map/ppermute | solution.py:197
  3.8 7.5 %collective-permute-start.1 = (bf16[8,4096]{1,0:T(8,128)(2,1)}, bf16[8,4096]{1,0:T(8,128)(2,1)S(1)}, u32[]{:S(2)}, u32[]{:S(2)}) collective-permute-start(bf16[8,4096]{1,0:T(8,128)(2,1)} %bitcast.34), channel_id=1, source_target_pairs={{0,16},{1,17},{2,18},{3,19},{4,20},{5,21},{6,22},{7,23},{8,24},{9,... | collective-permute-start | bytes 196616 | tf_op jit(solution)/shard_map/ppermute | solution.py:197
  6.4 6.3 %collective-permute-start.2 = (bf16[8,4096]{1,0:T(8,128)(2,1)}, bf16[8,4096]{1,0:T(8,128)(2,1)S(1)}, u32[]{:S(2)}, u32[]{:S(2)}) collective-permute-start(bf16[8,4096]{1,0:T(8,128)(2,1)} %bitcast.35), channel_id=1, source_target_pairs={{0,24},{1,25},{2,26},{3,27},{4,28},{5,29},{6,30},{7,31},{8,16},{9,... | collective-permute-start | bytes 196616 | tf_op jit(solution)/shard_map/ppermute | solution.py:197
  6.4 9.3 %collective-permute-start.5 = (bf16[8,4096]{1,0:T(8,128)(2,1)}, bf16[8,4096]{1,0:T(8,128)(2,1)S(1)}, u32[]{:S(2)}, u32[]{:S(2)}) collective-permute-start(bf16[8,4096]{1,0:T(8,128)(2,1)} %bitcast.36), channel_id=1, source_target_pairs={{0,6},{1,7},{2,4},{3,5},{4,2},{5,3},{6,0},{7,1},{8,14},{9,15},{10,... | collective-permute-start | bytes 196616 | tf_op jit(solution)/shard_map/ppermute | solution.py:197
  9.0 33.9 %collective-permute-start.14 = (bf16[2,64,4096]{2,1,0:T(8,128)(2,1)}, bf16[2,64,4096]{2,1,0:T(8,128)(2,1)S(1)}, u32[]{:S(2)}, u32[]{:S(2)}) collective-permute-start(bf16[2,64,4096]{2,1,0:T(8,128)(2,1)} %bitcast.32), channel_id=1, source_target_pairs={{0,1},{1,0},{2,3},{3,2},{4,5},{5,4},{6,7},{7,6},{8,9},{9,8},{10,11... | collective-permute-start | bytes 3145736 | tf_op jit(solution)/shard_map/ppermute | solution.py:197
  12.7 19.6 %collective-permute-start.3 = (bf16[32,4096]{1,0:T(8,128)(2,1)S(1)}, bf16[32,4096]{1,0:T(8,128)(2,1)S(1)}, u32[]{:S(2)}, u32[]{:S(2)}) collective-permute-start(bf16[32,4096]{1,0:T(8,128)(2,1)S(1)} %constant_dynamic-update-slice_fusion.refs_0_), channel_id=1, source_target_pairs={{0,2},{1,3},{2,0},{3,1},{4,6},{5,7},{6,4},{7,5},{8,10},{9,11},{10,... | collective-permute-start | bytes 786440 | tf_op jit(solution)/shard_map/ppermute | solution.py:197
  14.2 18.6 %collective-permute-start.4 = (bf16[32,4096]{1,0:T(8,128)(2,1)S(1)}, bf16[32,4096]{1,0:T(8,128)(2,1)S(1)}, u32[]{:S(2)}, u32[]{:S(2)}) collective-permute-start(bf16[32,4096]{1,0:T(8,128)(2,1)S(1)} %constant_dynamic-update-slice_fusion.refs_0_), channel_id=1, source_target_pairs={{0,4},{1,5},{2,6},{3,7},{4,0},{5,1},{6,2},{7,3},{8,12},{9,13},{10,... | collective-permute-start | bytes 786440 | tf_op jit(solution)/shard_map/ppermute | solution.py:197
  15.7 21.9 %collective-permute-start.9 = (bf16[32,4096]{1,0:T(8,128)(2,1)S(1)}, bf16[32,4096]{1,0:T(8,128)(2,1)S(1)}, u32[]{:S(2)}, u32[]{:S(2)}) collective-permute-start(bf16[32,4096]{1,0:T(8,128)(2,1)S(1)} %constant_dynamic-update-slice_fusion.refs_0_), channel_id=1, source_target_pairs={{0,1},{1,0},{2,3},{3,2},{4,5},{5,4},{6,7},{7,6},{8,9},{9,8},{10,11... | collective-permute-start | bytes 786440 | tf_op jit(solution)/shard_map/ppermute | solution.py:197
  26.2 6.1 %collective-permute-start.8 = (bf16[8,4096]{1,0:T(8,128)(2,1)S(1)}, bf16[8,4096]{1,0:T(8,128)(2,1)S(1)}, u32[]{:S(2)}, u32[]{:S(2)}) collective-permute-start(bf16[8,4096]{1,0:T(8,128)(2,1)S(1)} %collective-permute-done.5), channel_id=1, source_target_pairs={{0,24},{1,25},{2,26},{3,27},{4,28},{5,29},{6,30},{7,31},{8,16},{9,... | collective-permute-start | bytes 196616 | tf_op jit(solution)/shard_map/ppermute | solution.py:197
  43.6 8.3 %collective-permute-start.22 = (bf16[8,4096]{1,0:T(8,128)(2,1)S(1)}, bf16[8,4096]{1,0:T(8,128)(2,1)S(1)}, u32[]{:S(2)}, u32[]{:S(2)}) collective-permute-start(bf16[8,4096]{1,0:T(8,128)(2,1)S(1)} %get-tuple-element.78), channel_id=1, source_target_pairs={{0,24},{1,25},{2,26},{3,27},{4,28},{5,29},{6,30},{7,31},{8,16},{9,... | collective-permute-start | bytes 196616 | tf_op jit(solution)/shard_map/ppermute | solution.py:197
  45.5 7.1 %collective-permute-start.21 = (bf16[8,4096]{1,0:T(8,128)(2,1)S(1)}, bf16[8,4096]{1,0:T(8,128)(2,1)S(1)}, u32[]{:S(2)}, u32[]{:S(2)}) collective-permute-start(bf16[8,4096]{1,0:T(8,128)(2,1)S(1)} %get-tuple-element.79), channel_id=1, source_target_pairs={{0,16},{1,17},{2,18},{3,19},{4,20},{5,21},{6,22},{7,23},{8,24},{9,... | collective-permute-start | bytes 196616 | tf_op jit(solution)/shard_map/ppermute | solution.py:197
  45.5 7.1 %collective-permute-start.20 = (bf16[8,4096]{1,0:T(8,128)(2,1)S(1)}, bf16[8,4096]{1,0:T(8,128)(2,1)S(1)}, u32[]{:S(2)}, u32[]{:S(2)}) collective-permute-start(bf16[8,4096]{1,0:T(8,128)(2,1)S(1)} %get-tuple-element.77), channel_id=1, source_target_pairs={{0,8},{1,9},{2,10},{3,11},{4,12},{5,13},{6,14},{7,15},{8,0},{9,1},... | collective-permute-start | bytes 196616 | tf_op jit(solution)/shard_map/ppermute | solution.py:197
  48.1 8.4 %collective-permute-start.15 = (bf16[32,4096]{1,0:T(8,128)(2,1)S(1)}, bf16[32,4096]{1,0:T(8,128)(2,1)S(1)}, u32[]{:S(2)}, u32[]{:S(2)}) collective-permute-start(bf16[32,4096]{1,0:T(8,128)(2,1)S(1)} %get-tuple-element.81), channel_id=1, source_target_pairs={{0,2},{1,3},{2,0},{3,1},{4,6},{5,7},{6,4},{7,5},{8,10},{9,11},{10,... | collective-permute-start | bytes 786440 | tf_op jit(solution)/shard_map/ppermute | solution.py:197
  48.7 7.8 %collective-permute-start.16 = (bf16[32,4096]{1,0:T(8,128)(2,1)S(1)}, bf16[32,4096]{1,0:T(8,128)(2,1)S(1)}, u32[]{:S(2)}, u32[]{:S(2)}) collective-permute-start(bf16[32,4096]{1,0:T(8,128)(2,1)S(1)} %get-tuple-element.80), channel_id=1, source_target_pairs={{0,4},{1,5},{2,6},{3,7},{4,0},{5,1},{6,2},{7,3},{8,12},{9,13},{10,... | collective-permute-start | bytes 786440 | tf_op jit(solution)/shard_map/ppermute | solution.py:197
  52.6 11.0 %collective-permute-start.23 = (bf16[8,4096]{1,0:T(8,128)(2,1)S(1)}, bf16[8,4096]{1,0:T(8,128)(2,1)S(1)}, u32[]{:S(2)}, u32[]{:S(2)}) collective-permute-start(bf16[8,4096]{1,0:T(8,128)(2,1)S(1)} %add_convert_fusion.3), channel_id=1, source_target_pairs={{0,6},{1,7},{2,4},{3,5},{4,2},{5,3},{6,0},{7,1},{8,14},{9,15},{10,... | collective-permute-start | bytes 196616 | tf_op jit(solution)/shard_map/ppermute | solution.py:197
  56.6 7.1 %collective-permute-start.17 = (bf16[8,4096]{1,0:T(8,128)(2,1)S(1)}, bf16[8,4096]{1,0:T(8,128)(2,1)S(1)}, u32[]{:S(2)}, u32[]{:S(2)}) collective-permute-start(bf16[8,4096]{1,0:T(8,128)(2,1)S(1)} %get-tuple-element.87), channel_id=1, source_target_pairs={{0,8},{1,9},{2,10},{3,11},{4,12},{5,13},{6,14},{7,15},{8,0},{9,1},... | collective-permute-start | bytes 196616 | tf_op jit(solution)/shard_map/ppermute | solution.py:197
  57.3 6.4 %collective-permute-start.18 = (bf16[8,4096]{1,0:T(8,128)(2,1)S(1)}, bf16[8,4096]{1,0:T(8,128)(2,1)S(1)}, u32[]{:S(2)}, u32[]{:S(2)}) collective-permute-start(bf16[8,4096]{1,0:T(8,128)(2,1)S(1)} %get-tuple-element.86), channel_id=1, source_target_pairs={{0,16},{1,17},{2,18},{3,19},{4,20},{5,21},{6,22},{7,23},{8,24},{9,... | collective-permute-start | bytes 196616 | tf_op jit(solution)/shard_map/ppermute | solution.py:197
  59.0 6.2 %collective-permute-start.19 = (bf16[8,4096]{1,0:T(8,128)(2,1)S(1)}, bf16[8,4096]{1,0:T(8,128)(2,1)S(1)}, u32[]{:S(2)}, u32[]{:S(2)}) collective-permute-start(bf16[8,4096]{1,0:T(8,128)(2,1)S(1)} %get-tuple-element.85), channel_id=1, source_target_pairs={{0,24},{1,25},{2,26},{3,27},{4,28},{5,29},{6,30},{7,31},{8,16},{9,... | collective-permute-start | bytes 196616 | tf_op jit(solution)/shard_map/ppermute | solution.py:197
  65.3 6.2 %collective-permute-start.26 = (bf16[8,4096]{1,0:T(8,128)(2,1)S(1)}, bf16[8,4096]{1,0:T(8,128)(2,1)S(1)}, u32[]{:S(2)}, u32[]{:S(2)}) collective-permute-start(bf16[8,4096]{1,0:T(8,128)(2,1)S(1)} %fusion.11), channel_id=1, source_target_pairs={{0,24},{1,25},{2,26},{3,27},{4,28},{5,29},{6,30},{7,31},{8,16},{9,... | collective-permute-start | bytes 196616 | tf_op jit(solution)/shard_map/ppermute | solution.py:197
  72.8 13.1 %collective-permute-start.27 = (bf16[32,4096]{1,0:T(8,128)(2,1)S(1)}, bf16[32,4096]{1,0:T(8,128)(2,1)S(1)}, u32[]{:S(2)}, u32[]{:S(2)}) collective-permute-start(bf16[32,4096]{1,0:T(8,128)(2,1)S(1)} %pad_maximum_fusion.refs_0_), channel_id=1, source_target_pairs={{0,2},{1,3},{2,0},{3,1},{4,6},{5,7},{6,4},{7,5},{8,10},{9,11},{10,... | collective-permute-start | bytes 786440 | tf_op jit(solution)/shard_map/ppermute | solution.py:197
  75.4 11.1 %collective-permute-start.28 = (bf16[32,4096]{1,0:T(8,128)(2,1)S(1)}, bf16[32,4096]{1,0:T(8,128)(2,1)S(1)}, u32[]{:S(2)}, u32[]{:S(2)}) collective-permute-start(bf16[32,4096]{1,0:T(8,128)(2,1)S(1)} %pad_maximum_fusion.refs_0_), channel_id=1, source_target_pairs={{0,4},{1,5},{2,6},{3,7},{4,0},{5,1},{6,2},{7,3},{8,12},{9,13},{10,... | collective-permute-start | bytes 786440 | tf_op jit(solution)/shard_map/ppermute | solution.py:197
  75.4 14.0 %collective-permute-start.33 = (bf16[32,4096]{1,0:T(8,128)(2,1)S(1)}, bf16[32,4096]{1,0:T(8,128)(2,1)S(1)}, u32[]{:S(2)}, u32[]{:S(2)}) collective-permute-start(bf16[32,4096]{1,0:T(8,128)(2,1)S(1)} %pad_maximum_fusion.refs_0_), channel_id=1, source_target_pairs={{0,1},{1,0},{2,3},{3,2},{4,5},{5,4},{6,7},{7,6},{8,9},{9,8},{10,11... | collective-permute-start | bytes 786440 | tf_op jit(solution)/shard_map/ppermute | solution.py:197
  76.6 6.9 %collective-permute-start.31 = (bf16[8,4096]{1,0:T(8,128)(2,1)S(1)}, bf16[8,4096]{1,0:T(8,128)(2,1)S(1)}, u32[]{:S(2)}, u32[]{:S(2)}) collective-permute-start(bf16[8,4096]{1,0:T(8,128)(2,1)S(1)} %collective-permute-done.29), channel_id=1, source_target_pairs={{0,16},{1,17},{2,18},{3,19},{4,20},{5,21},{6,22},{7,23},{8,24},{9,... | collective-permute-start | bytes 196616 | tf_op jit(solution)/shard_map/ppermute | solution.py:197
  79.9 6.1 %collective-permute-start.32 = (bf16[8,4096]{1,0:T(8,128)(2,1)S(1)}, bf16[8,4096]{1,0:T(8,128)(2,1)S(1)}, u32[]{:S(2)}, u32[]{:S(2)}) collective-permute-start(bf16[8,4096]{1,0:T(8,128)(2,1)S(1)} %collective-permute-done.29), channel_id=1, source_target_pairs={{0,24},{1,25},{2,26},{3,27},{4,28},{5,29},{6,30},{7,31},{8,16},{9,... | collective-permute-start | bytes 196616 | tf_op jit(solution)/shard_map/ppermute | solution.py:197
  95.5 9.4 %collective-permute-start.45 = (bf16[8,4096]{1,0:T(8,128)(2,1)S(1)}, bf16[8,4096]{1,0:T(8,128)(2,1)S(1)}, u32[]{:S(2)}, u32[]{:S(2)}) collective-permute-start(bf16[8,4096]{1,0:T(8,128)(2,1)S(1)} %get-tuple-element.73), channel_id=1, source_target_pairs={{0,24},{1,25},{2,26},{3,27},{4,28},{5,29},{6,30},{7,31},{8,16},{9,... | collective-permute-start | bytes 196616 | tf_op jit(solution)/shard_map/ppermute | solution.py:197
  97.5 7.4 %collective-permute-start.44 = (bf16[8,4096]{1,0:T(8,128)(2,1)S(1)}, bf16[8,4096]{1,0:T(8,128)(2,1)S(1)}, u32[]{:S(2)}, u32[]{:S(2)}) collective-permute-start(bf16[8,4096]{1,0:T(8,128)(2,1)S(1)} %get-tuple-element.74), channel_id=1, source_target_pairs={{0,16},{1,17},{2,18},{3,19},{4,20},{5,21},{6,22},{7,23},{8,24},{9,... | collective-permute-start | bytes 196616 | tf_op jit(solution)/shard_map/ppermute | solution.py:197
  97.5 7.4 %collective-permute-start.43 = (bf16[8,4096]{1,0:T(8,128)(2,1)S(1)}, bf16[8,4096]{1,0:T(8,128)(2,1)S(1)}, u32[]{:S(2)}, u32[]{:S(2)}) collective-permute-start(bf16[8,4096]{1,0:T(8,128)(2,1)S(1)} %get-tuple-element.72), channel_id=1, source_target_pairs={{0,8},{1,9},{2,10},{3,11},{4,12},{5,13},{6,14},{7,15},{8,0},{9,1},... | collective-permute-start | bytes 196616 | tf_op jit(solution)/shard_map/ppermute | solution.py:197
  100.0 8.0 %collective-permute-start.38 = (bf16[32,4096]{1,0:T(8,128)(2,1)S(1)}, bf16[32,4096]{1,0:T(8,128)(2,1)S(1)}, u32[]{:S(2)}, u32[]{:S(2)}) collective-permute-start(bf16[32,4096]{1,0:T(8,128)(2,1)S(1)} %get-tuple-element.76), channel_id=1, source_target_pairs={{0,2},{1,3},{2,0},{3,1},{4,6},{5,7},{6,4},{7,5},{8,10},{9,11},{10,... | collective-permute-start | bytes 786440 | tf_op jit(solution)/shard_map/ppermute | solution.py:197
  102.0 8.8 %collective-permute-start.39 = (bf16[32,4096]{1,0:T(8,128)(2,1)S(1)}, bf16[32,4096]{1,0:T(8,128)(2,1)S(1)}, u32[]{:S(2)}, u32[]{:S(2)}) collective-permute-start(bf16[32,4096]{1,0:T(8,128)(2,1)S(1)} %get-tuple-element.75), channel_id=1, source_target_pairs={{0,4},{1,5},{2,6},{3,7},{4,0},{5,1},{6,2},{7,3},{8,12},{9,13},{10,... | collective-permute-start | bytes 786440 | tf_op jit(solution)/shard_map/ppermute | solution.py:197
  105.0 13.1 %collective-permute-start.46 = (bf16[8,4096]{1,0:T(8,128)(2,1)S(1)}, bf16[8,4096]{1,0:T(8,128)(2,1)S(1)}, u32[]{:S(2)}, u32[]{:S(2)}) collective-permute-start(bf16[8,4096]{1,0:T(8,128)(2,1)S(1)} %add_convert_fusion.2), channel_id=1, source_target_pairs={{0,6},{1,7},{2,4},{3,5},{4,2},{5,3},{6,0},{7,1},{8,14},{9,15},{10,... | collective-permute-start | bytes 196616 | tf_op jit(solution)/shard_map/ppermute | solution.py:197
  111.0 7.1 %collective-permute-start.40 = (bf16[8,4096]{1,0:T(8,128)(2,1)S(1)}, bf16[8,4096]{1,0:T(8,128)(2,1)S(1)}, u32[]{:S(2)}, u32[]{:S(2)}) collective-permute-start(bf16[8,4096]{1,0:T(8,128)(2,1)S(1)} %get-tuple-element.84), channel_id=1, source_target_pairs={{0,8},{1,9},{2,10},{3,11},{4,12},{5,13},{6,14},{7,15},{8,0},{9,1},... | collective-permute-start | bytes 196616 | tf_op jit(solution)/shard_map/ppermute | solution.py:197
  111.3 6.8 %collective-permute-start.41 = (bf16[8,4096]{1,0:T(8,128)(2,1)S(1)}, bf16[8,4096]{1,0:T(8,128)(2,1)S(1)}, u32[]{:S(2)}, u32[]{:S(2)}) collective-permute-start(bf16[8,4096]{1,0:T(8,128)(2,1)S(1)} %get-tuple-element.83), channel_id=1, source_target_pairs={{0,16},{1,17},{2,18},{3,19},{4,20},{5,21},{6,22},{7,23},{8,24},{9,... | collective-permute-start | bytes 196616 | tf_op jit(solution)/shard_map/ppermute | solution.py:197
  (17 other events, 76.0 us)
